TPU v7x, 32 devices: a whole 2x2x4 slice. The times are simulated.
32 devices in a mesh: ep: 32 (over z, y, x, core).
Axes of the slice: x: 2, y: 2, z: 4, core: 2. Of those that a mesh axis runs over, the one named last changes fastest.
Arguments:
- tokens: bfloat16 [4096, 2048], P('ep'), may hold values from -6 to 6
- norm_gain: float32 [2048], replicated, may hold values from 0.1 to 1.9
- expert_ids: int32 [4096, 4], P('ep'), may hold values from 0 to 63, as said below
- gate_weights: float32 [4096, 4], P('ep'), may hold values from 0.1 to 0.6
- expert_gate: bfloat16 [64, 2048, 512], P('ep'), may hold values from -0.125 to 0.125
- expert_up: bfloat16 [64, 2048, 512], P('ep'), may hold values from -0.125 to 0.125
- expert_down: bfloat16 [64, 512, 2048], P('ep'), may hold values from -0.25 to 0.25
- shared_gate: bfloat16 [2048, 512], P('ep'), may hold values from -0.125 to 0.125
- shared_up: bfloat16 [2048, 512], P('ep'), may hold values from -0.125 to 0.125
- shared_down: bfloat16 [512, 2048], P(None, 'ep'), may hold values from -0.25 to 0.25
Outputs:
- mixed: bfloat16 [4096, 2048], P('ep')
Inputs may be any that keep to these rules, and one draw needn't show every extreme that they name: `expert_ids`: expert e belongs to device e // 2; each row names 4 experts of 4 different devices; among the rows of one device at most 24 name experts of any one device, hence at most 24 any one expert; in every aligned block of 128 rows exactly 24 rows name one and the same expert.
All inputs are finite; a program needn't handle non-finite values.
Results may differ from a plain program's by a relative error of at most 0.0067.
Values may be sent and summed in bfloat16 or wider, within the bound.
A program may use at most 128 MiB of HBM per device.

v0:
```python
import functools

import jax
import jax.numpy as jnp
from jax import lax
from jax.experimental import pallas as pl
from jax.experimental.pallas import tpu as pltpu
from jax.sharding import PartitionSpec as P

EPS = 1e-06
GROUPS = 4
MESH = pl.DeviceIdType.MESH
ORDER = ((0, 1, 2, 3), (1, 0, 2, 3), (2, 3, 1, 0), (3, 2, 1, 0))
BACK = ((1, 2, 3), (2, 3, 0), (1, 0, 3), (2, 1, 0))


def normalize(tokens, norm_gain):
    values = tokens.astype(jnp.float32)
    scaled = values * lax.rsqrt(jnp.mean(values * values, axis=-1, keepdims=True) + EPS)
    return (scaled * norm_gain).astype(jnp.bfloat16)


def pick(table, row, column):
    value = jnp.int32(table[0][column])
    for i in range(1, len(table)):
        value = jnp.where(row == i, jnp.int32(table[i][column]), value)
    return value


def moe_kernel(
    plane, rows_sent, chunk,
    x_ref, pack_ref, unpack_ref, label_ref, weight_ref, slices_ref, gate_hbm, up_hbm, down_hbm,
    out_ref,
    gate, up, down, held, packed, got, back, above, below, partial, total, spread, shared,
    w_sem, zsend, zrecv, dsend, drecv, rsend, rrecv, psend, arecv, brecv,
    hzsend, hzrecv, hpsend, hprecv, hcsend, hcrecv,
):
    me = lax.axis_index("ep")
    z, p = me // plane, me % plane
    has_low, has_high = z > 0, z < GROUPS - 1
    rows = packed.shape[1] * packed.shape[2]
    part = shared.shape[1] // 3
    width = x_ref.shape[1]

    weights = [
        pltpu.make_async_copy(src, dst, w_sem.at[i])
        for i, (src, dst) in enumerate(((gate_hbm, gate), (up_hbm, up), (down_hbm, down)))
    ]
    for copy in weights:
        copy.start()

    back[...] = jnp.zeros_like(back)
    barrier = pltpu.get_barrier_semaphore()

    def greet(device):
        pl.semaphore_signal(barrier, inc=1, device_id=(device,), device_id_type=MESH)

    for i in range(1, plane):
        greet(z * plane + (p + i) % plane)

    for j in range(1, GROUPS):
        greet((z + j) % GROUPS * plane + p)
    pl.semaphore_wait(barrier, plane - 1 + GROUPS - 1)

    chips, chip, core = plane // 2, p // 2, p % 2

    def slice_copy(j):
        g = (z + j) % GROUPS
        return pltpu.make_async_remote_copy(
            src_ref=slices_ref.at[g], dst_ref=spread.at[core, chip, z],
            send_sem=hzsend.at[g], recv_sem=hzrecv.at[z],
            device_id=(g * plane + p,), device_id_type=MESH,
        )

    def slice_wait(j):
        g = (z + j) % GROUPS
        pltpu.make_async_remote_copy(
            src_ref=slices_ref.at[g], dst_ref=spread.at[core, chip, g],
            send_sem=hzsend.at[g], recv_sem=hzrecv.at[g],
            device_id=(g * plane + p,), device_id_type=MESH,
        ).wait_recv()

    def column_copy(i):
        return pltpu.make_async_remote_copy(
            src_ref=spread.at[core, chip], dst_ref=spread.at[core, chip],
            send_sem=hpsend.at[i], recv_sem=hprecv.at[i],
            device_id=(z * plane + (chip + i) % chips * 2 + core,), device_id_type=MESH,
        )

    def core_copy():
        return pltpu.make_async_remote_copy(
            src_ref=spread.at[core], dst_ref=spread.at[core],
            send_sem=hcsend.at[0], recv_sem=hcrecv.at[0],
            device_id=(me + 1 - 2 * core,), device_id_type=MESH,
        )

    for j in range(1, GROUPS):
        slice_copy(j).start()

    def along(src, g, direction):
        return pltpu.make_async_remote_copy(
            src_ref=src, dst_ref=held.at[g],
            send_sem=zsend.at[direction, g], recv_sem=zrecv.at[g],
            device_id=(me + (plane if direction else -plane),), device_id_type=MESH,
        )

    @pl.when(has_low)
    def _():
        along(x_ref, z, 0).start()

    @pl.when(has_high)
    def _():
        along(x_ref, z, 1).start()

    held[z] = x_ref[...]
    spread[core, chip, z] = slices_ref[z]

    def dispatch_copy(g, q, i):
        return pltpu.make_async_remote_copy(
            src_ref=packed.at[g, q, pl.ds(0, rows_sent)],
            dst_ref=got.at[g, p, pl.ds(0, rows_sent)],
            send_sem=dsend.at[g, i], recv_sem=drecv.at[g, i],
            device_id=(z * plane + q,), device_id_type=MESH,
        )

    def return_copy(g, q, i):
        return pltpu.make_async_remote_copy(
            src_ref=got.at[g, q, pl.ds(0, rows_sent)],
            dst_ref=back.at[g, p, pl.ds(0, rows_sent)],
            send_sem=rsend.at[g, i], recv_sem=rrecv.at[g, i],
            device_id=(z * plane + q,), device_id_type=MESH,
        )

    def dispatch(step):
        g = pick(ORDER, z, step)
        if step:
            along(held.at[g], g, 0).wait_recv()

            @pl.when(jnp.logical_and(g > z, has_low))
            def _():
                along(held.at[g], g, 0).start()

            @pl.when(jnp.logical_and(g < z, has_high))
            def _():
                along(held.at[g], g, 1).start()

        for c in range(0, width, chunk):
            columns = pl.ds(c, chunk)
            packed[g, :, :, columns] = (
                jnp.dot(pack_ref[g], held[g, :, columns], preferred_element_type=jnp.float32)
                .astype(jnp.bfloat16)
                .reshape(packed.shape[1], packed.shape[2], chunk)
            )
        for i in range(1, plane):
            dispatch_copy(g, (p + i) % plane, i).start()
        got[g, p] = packed[g, p]

    def compute(step):
        g = pick(ORDER, z, step)
        for i in range(1, plane):
            dispatch_copy(g, (p + i) % plane, i).wait_recv()
        x = got[g].reshape(rows, width)
        label = label_ref[g]
        hidden = []
        for e in range(gate.shape[0]):
            gate_val = jnp.dot(x, gate[e], preferred_element_type=jnp.float32)
            up_val = jnp.dot(x, up[e], preferred_element_type=jnp.float32)
            value = gate_val / (1.0 + jnp.exp(-gate_val)) * up_val
            hidden.append(jnp.where(label == e, value, 0.0).astype(jnp.bfloat16))
        for c in range(0, width, chunk):
            columns = pl.ds(c, chunk)
            value = jnp.zeros((rows, chunk), jnp.float32)
            for e in range(gate.shape[0]):
                value += jnp.dot(
                    hidden[e], down[e, :, columns], preferred_element_type=jnp.float32
                )
            got[g, :, :, columns] = (
                (value * weight_ref[g])
                .astype(jnp.bfloat16)
                .reshape(got.shape[1], got.shape[2], chunk)
            )
        for i in range(1, plane):
            return_copy(g, (p + i) % plane, i).start()
        back[g, p] = got[g, p]

    def partial_copy(g, upward):
        landing, sem = (below, brecv) if upward else (above, arecv)
        return pltpu.make_async_remote_copy(
            src_ref=partial.at[g], dst_ref=landing.at[g],
            send_sem=psend.at[g], recv_sem=sem.at[g],
            device_id=(me + (plane if upward else -plane),), device_id_type=MESH,
        )

    def combine(g):
        for i in range(1, plane):
            return_copy(g, (p + i) % plane, i).wait_recv()
        for c in range(0, width, chunk):
            columns = pl.ds(c, chunk)
            total[:, columns] = jnp.dot(
                unpack_ref[g],
                back[g, :, :, columns].reshape(rows, chunk),
                preferred_element_type=jnp.float32,
            )

        x = held[g]
        gate_val = jnp.dot(x, shared[:, :part], preferred_element_type=jnp.float32)
        up_val = jnp.dot(x, shared[:, part : 2 * part], preferred_element_type=jnp.float32)
        hidden = (gate_val / (1.0 + jnp.exp(-gate_val)) * up_val).astype(jnp.bfloat16)
        for c in range(0, width, chunk):
            total[:, c : c + chunk] += lax.dot_general(
                hidden, shared[c : c + chunk, 2 * part :], (((1,), (1,)), ((), ())),
                preferred_element_type=jnp.float32,
            )

        @pl.when(jnp.logical_and(g <= z, has_high))
        def _():
            partial_copy(g, False).wait_recv()
            total[...] += above[g].astype(jnp.float32)

        @pl.when(jnp.logical_and(g >= z, has_low))
        def _():
            partial_copy(g, True).wait_recv()
            total[...] += below[g].astype(jnp.float32)

    def pass_on(step):
        g = pick(BACK, z, step)
        combine(g)
        partial[g] = total[...].astype(jnp.bfloat16)

        @pl.when(g > z)
        def _():
            partial_copy(g, True).start()

        @pl.when(g < z)
        def _():
            partial_copy(g, False).start()

    dispatch(0)
    for j in range(1, GROUPS):
        slice_wait(j)
    for i in range(1, chips):
        column_copy(i).start()
    dispatch(1)
    for copy in weights:
        copy.wait()
    compute(0)
    dispatch(2)
    for i in range(1, chips):
        column_copy(i).wait_recv()
    core_copy().start()
    compute(1)
    dispatch(3)
    pltpu.make_async_remote_copy(
        src_ref=spread.at[core], dst_ref=spread.at[1 - core],
        send_sem=hcsend.at[0], recv_sem=hcrecv.at[0],
        device_id=(me + 1 - 2 * core,), device_id_type=MESH,
    ).wait_recv()
    piece = spread.shape[3]

    def lay(index, _):
        g, q = index // plane, index % plane
        start = pl.multiple_of(index * piece, piece)
        shared[pl.ds(start, piece), :] = spread[q % 2, q // 2, g]
        return 0

    lax.fori_loop(0, GROUPS * plane, lay, 0)
    compute(2)
    at_end = jnp.logical_not(jnp.logical_and(has_low, has_high))

    @pl.when(at_end)
    def _():
        pass_on(0)

    compute(3)

    @pl.when(jnp.logical_not(at_end))
    def _():
        pass_on(0)

    for step in range(1, GROUPS - 1):
        pass_on(step)
    combine(z)
    out_ref[...] = total[...].astype(out_ref.dtype)

    for j in range(1, GROUPS):
        slice_copy(j).wait_send()
    for i in range(1, chips):
        column_copy(i).wait_send()
    core_copy().wait_send()

    for g in range(GROUPS):
        for i in range(1, plane):
            q = (p + i) % plane
            dispatch_copy(g, q, i).wait_send()
            return_copy(g, q, i).wait_send()

        @pl.when(jnp.logical_and(g >= z, has_low))
        def _():
            along(held.at[g], g, 0).wait_send()

        @pl.when(jnp.logical_and(g <= z, has_high))
        def _():
            along(held.at[g], g, 1).wait_send()

        @pl.when(g != z)
        def _():
            partial_copy(g, True).wait_send()


def mixed_sum(
    normed, pack, unpack, label, weight, slices, expert_gate, expert_up, expert_down, capacity
):
    count_tok, width = normed.shape
    groups, rows, _ = pack.shape
    plane = lax.axis_size("ep") // groups
    padded = rows // plane
    bf16 = jnp.bfloat16
    rows_sent = -(-capacity // 8) * 8
    blocks = (groups, plane, padded, width)
    whole = (groups, count_tok, width)
    dma = pltpu.SemaphoreType.DMA
    vmem = pl.BlockSpec(memory_space=pltpu.VMEM)
    hbm = pl.BlockSpec(memory_space=pl.ANY)
    return pl.pallas_call(
        functools.partial(moe_kernel, plane, rows_sent, width // 4),
        out_shape=jax.ShapeDtypeStruct((count_tok, width), bf16),
        in_specs=[vmem] * 6 + [hbm] * 3,
        out_specs=vmem,
        scratch_shapes=[
            pltpu.VMEM(expert_gate.shape, bf16),
            pltpu.VMEM(expert_up.shape, bf16),
            pltpu.VMEM(expert_down.shape, bf16),
            pltpu.VMEM(whole, bf16),
            pltpu.VMEM(blocks, bf16),
            pltpu.VMEM(blocks, bf16),
            pltpu.VMEM(blocks, bf16),
            pltpu.VMEM(whole, bf16),
            pltpu.VMEM(whole, bf16),
            pltpu.VMEM(whole, bf16),
            pltpu.VMEM((count_tok, width), jnp.float32),
            pltpu.VMEM((2, plane // 2) + slices.shape, bf16),
            pltpu.VMEM((width, slices.shape[2]), bf16),
            dma((3,)),
            dma((2, groups)),
            dma((groups,)),
            dma((groups, plane)),
            dma((groups, plane)),
            dma((groups, plane)),
            dma((groups, plane)),
            dma((groups,)),
            dma((groups,)),
            dma((groups,)),
            dma((groups,)),
            dma((groups,)),
            dma((plane // 2,)),
            dma((plane // 2,)),
            dma((1,)),
            dma((1,)),
        ],
        compiler_params=pltpu.CompilerParams(
            collective_id=0, has_side_effects=True, vmem_limit_bytes=60 * 1024 * 1024
        ),
    )(normed, pack, unpack, label, weight, slices, expert_gate, expert_up, expert_down)


def spread_kernel(n, x_ref, out_ref, landed, send_sem, recv_sem):
    me = lax.axis_index("ep")
    barrier = pltpu.get_barrier_semaphore()
    for i in range(1, n):
        pl.semaphore_signal(barrier, inc=1, device_id=((me + i) % n,), device_id_type=MESH)
    pl.semaphore_wait(barrier, n - 1)

    def copy(i):
        return pltpu.make_async_remote_copy(
            src_ref=x_ref, dst_ref=landed.at[me],
            send_sem=send_sem.at[i], recv_sem=recv_sem.at[i],
            device_id=((me + i) % n,), device_id_type=MESH,
        )

    for i in range(1, n):
        copy(i).start()
    landed[me] = x_ref[...]
    for i in range(1, n):
        copy(i).wait_recv()
    out_ref[...] = landed[...]
    for i in range(1, n):
        copy(i).wait_send()


def gather_small(x):
    n = lax.axis_size("ep")
    vmem = pl.BlockSpec(memory_space=pltpu.VMEM)
    return pl.pallas_call(
        functools.partial(spread_kernel, n),
        out_shape=jax.ShapeDtypeStruct((n,) + x.shape, x.dtype),
        in_specs=[vmem],
        out_specs=vmem,
        scratch_shapes=[
            pltpu.VMEM((n,) + x.shape, x.dtype),
            pltpu.SemaphoreType.DMA((n,)),
            pltpu.SemaphoreType.DMA((n,)),
        ],
        compiler_params=pltpu.CompilerParams(collective_id=1, has_side_effects=True),
    )(x)


def per_device(
    tokens, norm_gain, expert_ids, gate_weights, expert_gate, expert_up, expert_down,
    shared_gate, shared_up, shared_down,
):
    f32, bf16 = jnp.float32, jnp.bfloat16
    normed = normalize(tokens, norm_gain)
    count_tok, top = expert_ids.shape
    local_experts = expert_gate.shape[0]
    devices = lax.axis_size("ep")
    plane = devices // GROUPS
    mean_rows = count_tok * top // devices
    capacity = mean_rows + mean_rows // 2
    padded = -(-capacity // 16) * 16
    me = lax.axis_index("ep")
    z, p = me // plane, me % plane

    small = jnp.concatenate([expert_ids.T.astype(f32), gate_weights.T], axis=0)
    small = gather_small(small)
    ids = small[:, :top].astype(jnp.int32)
    weights = small[:, top:]
    target = ids // local_experts
    slots = jnp.arange(padded, dtype=f32)
    earlier = jnp.tril(jnp.ones((count_tok, count_tok), bf16), -1)

    column = lax.dynamic_slice_in_dim(
        target.reshape(GROUPS, plane, top, count_tok), p, 1, axis=1
    )[:, 0]
    here = z * plane + jnp.arange(plane, dtype=jnp.int32)
    named = jnp.any(column[:, None] == here[:, None, None], axis=2)
    rank = jnp.einsum("ut,gqt->gqu", earlier, named.astype(bf16), preferred_element_type=f32)
    rank = jnp.where(named, rank, -1.0)
    pack = (rank[:, :, None, :] == slots[:, None]).astype(bf16)
    pack = pack.reshape(GROUPS, plane * padded, count_tok)
    unpack = (rank.transpose(0, 2, 1)[:, :, :, None] == slots).astype(bf16)
    unpack = unpack.reshape(GROUPS, count_tok, plane * padded)

    mine = target == me
    came = jnp.any(mine, axis=1)
    rank_in = jnp.einsum("ut,st->su", earlier, came.astype(bf16), preferred_element_type=f32)
    rank_in = jnp.where(came, rank_in, -1.0)
    slot_of = rank_in[:, None, :] == slots[:, None]
    which = jnp.sum(jnp.where(mine, ids % local_experts + 1, 0), axis=1)
    scale = jnp.sum(jnp.where(mine, weights, 0.0), axis=1)
    label = jnp.sum(jnp.where(slot_of, which[:, None, :], 0), axis=2) - 1
    weight = jnp.sum(jnp.where(slot_of, scale[:, None, :], 0.0), axis=2)
    label = label.reshape(GROUPS, plane * padded, 1)
    weight = weight.reshape(GROUPS, plane * padded, 1)

    depth = shared_gate.shape[0]
    slices = jnp.concatenate(
        [w.reshape(depth, GROUPS, -1) for w in (shared_gate, shared_up, shared_down.T)], axis=2
    ).transpose(1, 0, 2)
    return mixed_sum(
        normed, pack, unpack, label, weight, slices, expert_gate, expert_up, expert_down, capacity
    )


def solution(mesh):
    return jax.shard_map(
        per_device,
        mesh=mesh,
        in_specs=(
            P("ep", None),
            P(),
            P("ep", None),
            P("ep", None),
            P("ep", None, None),
            P("ep", None, None),
            P("ep", None, None),
            P("ep", None),
            P("ep", None),
            P(None, "ep"),
        ),
        out_specs=P("ep", None),
        check_vma=False,
    )
```

profile of v0, /device:TPU:0, one launch (start us, length us, event | category | flops | bytes accessed | tf_op | source)
XLA Modules:
  0.0 154.4 jit_solution(12070088110264540290)
XLA Ops:
  0.0 0.0 copy-start
  0.0 0.0 copy-start.3
  0.0 0.0 copy-start.2
  0.0 0.0 copy-start.1
  0.0 0.0 copy-start.4
  0.0 0.8 convert_bitcast_fusion
  0.8 1.3 pad_maximum_fusion.x_ref
  2.1 11.8 %shard_map.100 = f32[32,8,128]{2,1,0:T(8,128)} custom-call(f32[8,128]{1,0:T(8,128)} %pad_maximum_fusion.x_ref), custom_call_target="tpu_custom_call" | custom-call | tf_op jit(solution)/shard_map/pallas_call | solution.py:393
  13.9 1.1 select_reduce_fusion.2
  15.1 0.1 compare_reduce_fusion
  15.2 0.2 convolution_select_fusion.1
  15.3 0.1 eq.88
  15.4 0.2 copy.18
  15.6 0.1 eq.85
  15.7 0.8 compare_convert_fusion.unpack_ref
  16.5 0.8 fusion.3.pack_ref
  17.3 0.1 reduce_or.19
  17.3 0.2 convolution_select_fusion
  17.5 1.0 fusion.6
  18.6 0.6 select_reduce_fusion.1
  19.2 1.3 sub.20.label_ref
  20.6 0.2 select_reduce_fusion
  20.8 1.4 reshape.58.weight_ref
  22.1 0.0 copy-done
  22.1 0.0 copy-done.3
  22.2 0.0 copy-done.2
  22.2 0.7 maximum_bitcast_fusion.slices_ref
  22.9 0.0 copy-done.1
  22.9 0.2 fusion
  23.1 0.0 copy-done.4
  23.1 1.0 fusion.2.x_ref
  24.1 128.5 %shard_map.101 = bf16[128,2048]{1,0:T(8,128)(2,1)} custom-call(bf16[128,2048]{1,0:T(8,128)(2,1)} %fusion.2.x_ref, bf16[4,256,128]{2,1,0:T(8,128)(2,1)} %fusion.3.pack_ref, bf16[4,128,256]{2,1,0:T(8,128)(2,1)} %compare_convert_fusion.unpack_ref, s32[4,256,1]{2,1,0:T(8,128)} %sub.20.label_ref, f32[4,256,1]{2,1,0:T(8,128)} %reshape.58.weight_ref, ...), custom_call_target="tpu_custom_call" | custom-call | tf_op jit(solution)/shard_map/pallas_call | solution.py:324
  152.6 1.9 %copy.31 = bf16[128,2048]{1,0:T(8,128)(2,1)} copy(bf16[128,2048]{1,0:T(8,128)(2,1)} %shard_map.101) | data formatting | bytes 1048576
  (8 shorter events, 0.1 us)
Async XLA Ops:
  0.0 22.1 %copy-start = (bf16[64,512]{1,0:T(8,128)(2,1)S(1)}, bf16[64,512]{1,0:T(8,128)(2,1)}, u32[]{:S(2)}) copy-start(bf16[64,512]{1,0:T(8,128)(2,1)} %param.18) | copy-start | bytes 196612
  0.0 22.1 %copy-start.3 = (bf16[512,64]{0,1:T(8,128)(2,1)S(1)}, bf16[512,64]{0,1:T(8,128)(2,1)}, u32[]{:S(2)}) copy-start(bf16[512,64]{0,1:T(8,128)(2,1)} %param.19) | copy-start | bytes 196612
  0.0 22.2 %copy-start.2 = (bf16[64,512]{1,0:T(8,128)(2,1)S(1)}, bf16[64,512]{1,0:T(8,128)(2,1)}, u32[]{:S(2)}) copy-start(bf16[64,512]{1,0:T(8,128)(2,1)} %param.17) | copy-start | bytes 196612
  0.0 22.9 %copy-start.1 = (bf16[128,2048]{1,0:T(8,128)(2,1)S(1)}, bf16[128,2048]{1,0:T(8,128)(2,1)}, u32[]{:S(2)}) copy-start(bf16[128,2048]{1,0:T(8,128)(2,1)} %param.10) | copy-start | bytes 1572868
  0.0 23.1 %copy-start.4 = (f32[2048]{0:T(1024)S(1)}, f32[2048]{0:T(1024)}, u32[]{:S(2)}) copy-start(f32[2048]{0:T(1024)} %param.11) | copy-start | bytes 24580
where the time goes:
time: 155 us; the launch traced here: 154 us
  Pallas kernels  140 us (90%)
  other arithmetic  8.65 us (6%)
  local copies, waits for them, and re-layouts  4.97 us (3%)
    pallas_call x1, Pallas kernels, mixed_sum(): pl.pallas_call(functools.partial(moe_kernel, plane, rows_sent, width // 4...  128 us
    pallas_call x1, Pallas kernels, gather_small(): pl.pallas_call(functools.partial(spread_kernel, n), out_shape=jax.ShapeDt...  11.8 us

commit v1 on v0

v1 whole, which is shorter than its diff:
```python
import functools

import jax
import jax.numpy as jnp
from jax import lax
from jax.experimental import pallas as pl
from jax.experimental.pallas import tpu as pltpu
from jax.sharding import PartitionSpec as P

EPS = 1e-06
GROUPS = 4
CHUNKS = 4
MESH = pl.DeviceIdType.MESH
ORDER = ((0, 1, 2, 3), (1, 2, 3, 0), (2, 1, 0, 3), (3, 2, 1, 0))
BACK = ((1, 2, 3), (3, 2, 0), (0, 1, 3), (2, 1, 0))
GOAL = ((1, 1, 2), (3, 2, 0), (0, 1, 3), (2, 2, 1))
SLOT = ((0, 2, 3), (1, 1, 0), (1, 1, 0), (0, 2, 3))


def pick(table, row, column):
    value = jnp.int32(table[0][column])
    for i in range(1, len(table)):
        value = jnp.where(row == i, jnp.int32(table[i][column]), value)
    return value


def stack_rows(rank, slots):
    slot = lax.broadcasted_iota(jnp.int32, (slots, rank.shape[1]), 0).astype(jnp.float32)
    return [rank[q : q + 1, :] == slot for q in range(rank.shape[0])]


def moe_kernel(
    plane, slots, local,
    tok_ref, gain_ref, ids_ref, wts_ref, sgate_ref, sup_ref, sdown_ref,
    gate_hbm, up_hbm, down_hbm,
    out_ref,
    gate, up, down, held, pack, packed, got, back, partial, land, route, slices, spread, hidden_s,
    w_sem, rsend, rrecv, fsend, frecv, hzsend, hzrecv, hpsend, hprecv, hcsend, hcrecv,
    zsend, zrecv, dsend, drecv, bsend, brecv, lsend, lrecv,
):
    f32, bf16 = jnp.float32, jnp.bfloat16
    me = lax.axis_index("ep")
    z, p = me // plane, me % plane
    chips, chip, core = plane // 2, p // 2, p % 2
    has_low, has_high = z > 0, z < GROUPS - 1
    middle = jnp.logical_and(has_low, has_high)
    outer = jnp.logical_not(middle)
    count_tok, width = tok_ref.shape
    top = ids_ref.shape[0]
    rows = plane * slots
    part = sgate_ref.shape[1] // GROUPS
    chunk = width // CHUNKS

    weights = [
        pltpu.make_async_copy(src, dst, w_sem.at[i])
        for i, (src, dst) in enumerate(((gate_hbm, gate), (up_hbm, up), (down_hbm, down)))
    ]
    for copy in weights:
        copy.start()

    barrier = pltpu.get_barrier_semaphore()

    def greet(device):
        pl.semaphore_signal(barrier, inc=1, device_id=(device,), device_id_type=MESH)

    for i in range(1, plane):
        greet(z * plane + (p + i) % plane)
    for j in range(1, GROUPS):
        greet((z + j) % GROUPS * plane + p)

    for g in range(GROUPS):
        for i, ref in enumerate((sgate_ref, sup_ref, sdown_ref)):
            slices[g, :, i * part : (i + 1) * part] = ref[:, g * part : (g + 1) * part]
    route[z, p, :top, :] = ids_ref[...].astype(f32)
    route[z, p, top:, :] = wts_ref[...]
    values = tok_ref[...].astype(f32)
    scaled = values * lax.rsqrt(jnp.mean(values * values, axis=-1, keepdims=True) + EPS)
    held[z] = (scaled * gain_ref[...]).astype(bf16)
    spread[z, chip, core] = slices[z]

    before = (
        lax.broadcasted_iota(jnp.int32, (count_tok, count_tok), 0)
        < lax.broadcasted_iota(jnp.int32, (count_tok, count_tok), 1)
    ).astype(bf16)

    def ranks(named):
        rank = jnp.dot(named.astype(bf16), before, preferred_element_type=f32)
        return jnp.where(named, rank, -1.0)

    def make_pack(g):
        first = (
            (lax.broadcasted_iota(jnp.int32, (plane, count_tok), 0) + z * plane) * local
        ).astype(f32)
        named = jnp.zeros((plane, count_tok), jnp.bool_)
        for k in range(top):
            ids = route[g, p, k : k + 1, :]
            named = jnp.logical_or(
                named, jnp.logical_and(ids >= first, ids < first + float(local))
            )
        blocks = stack_rows(ranks(named), slots)
        pack[g] = jnp.concatenate([b.astype(f32) for b in blocks], axis=0).astype(bf16)

    def fill(g):
        for c in range(0, width, chunk):
            columns = pl.ds(c, chunk)
            packed[g, :, :, columns] = (
                jnp.dot(pack[g], held[g, :, columns], preferred_element_type=f32)
                .astype(bf16)
                .reshape(plane, slots, chunk)
            )

    make_pack(z)
    fill(z)
    pl.semaphore_wait(barrier, plane - 1 + GROUPS - 1)

    def route_copy(j, g):
        return pltpu.make_async_remote_copy(
            src_ref=route.at[g, p], dst_ref=route.at[g, p],
            send_sem=rsend.at[j], recv_sem=rrecv.at[g],
            device_id=((z + j) % GROUPS * plane + p,), device_id_type=MESH,
        )

    def route_forward(i, q):
        return pltpu.make_async_remote_copy(
            src_ref=route.at[:, q], dst_ref=route.at[:, q],
            send_sem=fsend.at[i], recv_sem=frecv.at[q],
            device_id=(z * plane + (p + i) % plane,), device_id_type=MESH,
        )

    def slice_copy(j):
        g = (z + j) % GROUPS
        return pltpu.make_async_remote_copy(
            src_ref=slices.at[g], dst_ref=spread.at[z, chip, core],
            send_sem=hzsend.at[j], recv_sem=hzrecv.at[z],
            device_id=(g * plane + p,), device_id_type=MESH,
        )

    def slice_wait(j):
        g = (z + j) % GROUPS
        pltpu.make_async_remote_copy(
            src_ref=slices.at[g], dst_ref=spread.at[g, chip, core],
            send_sem=hzsend.at[j], recv_sem=hzrecv.at[g],
            device_id=(g * plane + p,), device_id_type=MESH,
        ).wait_recv()

    def column_copy(i, g, c):
        return pltpu.make_async_remote_copy(
            src_ref=spread.at[g, c, core], dst_ref=spread.at[g, c, core],
            send_sem=hpsend.at[i, g], recv_sem=hprecv.at[c, g],
            device_id=(z * plane + (chip + i) % chips * 2 + core,), device_id_type=MESH,
        )

    def core_copy(c):
        return pltpu.make_async_remote_copy(
            src_ref=spread.at[:, :, c], dst_ref=spread.at[:, :, c],
            send_sem=hcsend.at[0], recv_sem=hcrecv.at[0],
            device_id=(me + 1 - 2 * core,), device_id_type=MESH,
        )

    def along(src, g, direction):
        return pltpu.make_async_remote_copy(
            src_ref=src, dst_ref=held.at[g],
            send_sem=zsend.at[direction, g], recv_sem=zrecv.at[g],
            device_id=(me + (plane if direction else -plane),), device_id_type=MESH,
        )

    def arrive(g):
        along(held.at[g], g, 0).wait_recv()

        @pl.when(jnp.logical_and(g > z, has_low))
        def _():
            along(held.at[g], g, 0).start()

        @pl.when(jnp.logical_and(g < z, has_high))
        def _():
            along(held.at[g], g, 1).start()

    def dispatch_copy(g, q, i):
        return pltpu.make_async_remote_copy(
            src_ref=packed.at[g, q], dst_ref=got.at[g, p],
            send_sem=dsend.at[g, i], recv_sem=drecv.at[g, i],
            device_id=(z * plane + q,), device_id_type=MESH,
        )

    def return_copy(g, q, i, c):
        columns = pl.ds(c * chunk, chunk)
        return pltpu.make_async_remote_copy(
            src_ref=got.at[g, q, :, columns], dst_ref=back.at[g, p, :, columns],
            send_sem=bsend.at[g, i, c], recv_sem=brecv.at[g, i, c],
            device_id=(z * plane + q,), device_id_type=MESH,
        )

    def dispatch(g):
        for i in range(1, plane):
            dispatch_copy(g, (p + i) % plane, i).start()
        got[g, p] = packed[g, p]

    def give_back(g, c):
        for i in range(1, plane):
            return_copy(g, (p + i) % plane, i, c).start()

    def labels(g):
        came = jnp.zeros((plane, count_tok), jnp.bool_)
        which = jnp.zeros((plane, count_tok), f32)
        scale = jnp.zeros((plane, count_tok), f32)
        first = (me * local).astype(f32)
        for k in range(top):
            ids = route[g, :, k, :] - first
            mine = jnp.logical_and(ids >= 0.0, ids < float(local))
            came = jnp.logical_or(came, mine)
            which += jnp.where(mine, ids + 1.0, 0.0)
            scale += jnp.where(mine, route[g, :, top + k, :], 0.0)
        blocks = stack_rows(ranks(came), slots)
        label, weight = [], []
        for q, block in enumerate(blocks):
            label.append(
                jnp.sum(jnp.where(block, which[q : q + 1, :], 0.0), axis=1, keepdims=True)
            )
            weight.append(
                jnp.sum(jnp.where(block, scale[q : q + 1, :], 0.0), axis=1, keepdims=True)
            )
        return jnp.concatenate(label, axis=0) - 1.0, jnp.concatenate(weight, axis=0)

    def compute(g, send):
        label, weight = labels(g)
        for i in range(1, plane):
            dispatch_copy(g, (p + i) % plane, i).wait_recv()
        x = got[g].reshape(rows, width)
        hidden = []
        for e in range(local):
            gate_val = jnp.dot(x, gate[e], preferred_element_type=f32)
            up_val = jnp.dot(x, up[e], preferred_element_type=f32)
            value = gate_val / (1.0 + jnp.exp(-gate_val)) * up_val
            hidden.append(jnp.where(label == float(e), value, 0.0).astype(bf16))
        for c in range(CHUNKS):
            columns = pl.ds(c * chunk, chunk)
            value = jnp.zeros((rows, chunk), f32)
            for e in range(local):
                value += jnp.dot(hidden[e], down[e, :, columns], preferred_element_type=f32)
            got[g, :, :, columns] = (value * weight).astype(bf16).reshape(plane, slots, chunk)
            if send is not None:

                @pl.when(send)
                def _():
                    give_back(g, c)

        back[g, p] = got[g, p]

    def combined(g, c):
        columns = pl.ds(c * chunk, chunk)
        for i in range(1, plane):
            return_copy(g, (p + i) % plane, i, c).wait_recv()
        total = lax.dot_general(
            pack[g], back[g, :, :, columns].reshape(rows, chunk), (((0,), (0,)), ((), ())),
            preferred_element_type=f32,
        )
        blocks = chunk // sgate_ref.shape[0]
        first = c * blocks
        down_t = spread[:, :, :, :, 2 * part :].reshape(width, part)[first * sgate_ref.shape[0] :][
            :chunk
        ]
        return total + lax.dot_general(
            hidden_s[g], down_t, (((1,), (1,)), ((), ())), preferred_element_type=f32
        )

    def land_copy(k, slot, goal, g, c):
        columns = pl.ds(c * chunk, chunk)
        return pltpu.make_async_remote_copy(
            src_ref=partial.at[g, :, columns], dst_ref=land.at[slot, :, columns],
            send_sem=lsend.at[k, c], recv_sem=lrecv.at[slot, c],
            device_id=(goal * plane + p,), device_id_type=MESH,
        )

    def pass_on(k):
        g = pick(BACK, z, k)
        slot, goal = pick(SLOT, z, k), pick(GOAL, z, k)
        for c in range(CHUNKS):
            columns = pl.ds(c * chunk, chunk)
            total = combined(g, c)
            if k:

                @pl.when(middle)
                def _():
                    land_copy(k, jnp.int32(k + 1), goal, g, c).wait_recv()
                    partial[g, :, columns] = (
                        total + land[k + 1, :, columns].astype(f32)
                    ).astype(bf16)

                @pl.when(outer)
                def _():
                    partial[g, :, columns] = total.astype(bf16)
            else:
                partial[g, :, columns] = total.astype(bf16)
            land_copy(k, slot, goal, g, c).start()

    for j in range(1, GROUPS):
        route_copy(j, z).start()
    for j in range(1, GROUPS):
        slice_copy(j).start()

    @pl.when(has_low)
    def _():
        along(held.at[z], z, 0).start()

    @pl.when(has_high)
    def _():
        along(held.at[z], z, 1).start()

    for i in range(1, chips):
        column_copy(i, z, chip).start()
    dispatch(z)
    for j in range(1, GROUPS):
        route_copy(j, (z + j) % GROUPS).wait_recv()
    for i in range(1, plane):
        route_forward(i, p).start()
    for j in range(1, GROUPS):
        slice_wait(j)
    for i in range(1, chips):
        for j in range(1, GROUPS):
            column_copy(i, (z + j) % GROUPS, chip).start()
    for j in range(1, GROUPS):
        make_pack((z + j) % GROUPS)

    one, two, three = (pick(ORDER, z, k) for k in range(1, GROUPS))
    arrive(one)

    @pl.when(middle)
    def _():
        arrive(three)

    fill(one)
    dispatch(one)
    for i in range(1, plane):
        route_forward(i, (p + i) % plane).wait_recv()
    for copy in weights:
        copy.wait()
    compute(z, None)
    arrive(two)
    fill(two)
    dispatch(two)
    compute(one, outer)

    @pl.when(outer)
    def _():
        arrive(three)

    fill(three)
    dispatch(three)
    for i in range(1, chips):
        for g in range(GROUPS):
            column_copy(i, g, (chip + i) % chips).wait_recv()
    core_copy(core).start()
    compute(two, jnp.logical_or(middle, outer))

    @pl.when(middle)
    def _():
        for c in range(CHUNKS):
            give_back(one, c)

    core_copy(1 - core).wait_recv()
    pre = jnp.dot(
        held[...].reshape(GROUPS * count_tok, width),
        spread[:, :, :, :, : 2 * part].reshape(width, 2 * part),
        preferred_element_type=f32,
    )
    gate_val, up_val = pre[:, :part], pre[:, part:]
    hidden_s[...] = (
        (gate_val / (1.0 + jnp.exp(-gate_val)) * up_val)
        .astype(bf16)
        .reshape(GROUPS, count_tok, part)
    )

    pass_on(0)
    compute(three, jnp.logical_or(middle, outer))
    for c in range(CHUNKS):
        give_back(z, c)
    pass_on(1)
    pass_on(2)
    for c in range(CHUNKS):
        columns = pl.ds(c * chunk, chunk)
        total = combined(z, c)
        for slot in range(2):
            land_copy(0, jnp.int32(slot), z, z, c).wait_recv()
            total += land[slot, :, columns].astype(f32)
        out_ref[:, columns] = total.astype(out_ref.dtype)

    for j in range(1, GROUPS):
        route_copy(j, z).wait_send()
        slice_copy(j).wait_send()
    for i in range(1, plane):
        route_forward(i, p).wait_send()
    for i in range(1, chips):
        for g in range(GROUPS):
            column_copy(i, g, chip).wait_send()
    core_copy(core).wait_send()
    for g in range(GROUPS):
        for i in range(1, plane):
            q = (p + i) % plane
            dispatch_copy(g, q, i).wait_send()
            for c in range(CHUNKS):
                return_copy(g, q, i, c).wait_send()

        @pl.when(jnp.logical_and(g >= z, has_low))
        def _():
            along(held.at[g], g, 0).wait_send()

        @pl.when(jnp.logical_and(g <= z, has_high))
        def _():
            along(held.at[g], g, 1).wait_send()

    for k in range(GROUPS - 1):
        for c in range(CHUNKS):
            land_copy(k, pick(SLOT, z, k), pick(GOAL, z, k), pick(BACK, z, k), c).wait_send()


def per_device(
    tokens, norm_gain, expert_ids, gate_weights, expert_gate, expert_up, expert_down,
    shared_gate, shared_up, shared_down,
):
    bf16, f32 = jnp.bfloat16, jnp.float32
    count_tok, width = tokens.shape
    top = expert_ids.shape[1]
    local = expert_gate.shape[0]
    devices = lax.axis_size("ep")
    plane = devices // GROUPS
    mean_rows = count_tok * top // devices
    capacity = mean_rows + mean_rows // 2
    slots = -(-capacity // 8) * 8
    rows = plane * slots
    depth, hidden = shared_gate.shape
    part = hidden // GROUPS
    dma = pltpu.SemaphoreType.DMA
    vmem = pl.BlockSpec(memory_space=pltpu.VMEM)
    hbm = pl.BlockSpec(memory_space=pl.ANY)
    blocks = (GROUPS, plane, slots, width)
    whole = (GROUPS, count_tok, width)
    return pl.pallas_call(
        functools.partial(moe_kernel, plane, slots, local),
        out_shape=jax.ShapeDtypeStruct((count_tok, width), bf16),
        in_specs=[vmem] * 7 + [hbm] * 3,
        out_specs=vmem,
        scratch_shapes=[
            pltpu.VMEM(expert_gate.shape, bf16),
            pltpu.VMEM(expert_up.shape, bf16),
            pltpu.VMEM(expert_down.shape, bf16),
            pltpu.VMEM(whole, bf16),
            pltpu.VMEM((GROUPS, rows, count_tok), bf16),
            pltpu.VMEM(blocks, bf16),
            pltpu.VMEM(blocks, bf16),
            pltpu.VMEM(blocks, bf16),
            pltpu.VMEM(whole, bf16),
            pltpu.VMEM(whole, bf16),
            pltpu.VMEM((GROUPS, plane, 2 * top, count_tok), f32),
            pltpu.VMEM((GROUPS, depth, 3 * part), bf16),
            pltpu.VMEM((GROUPS, plane // 2, 2, depth, 3 * part), bf16),
            pltpu.VMEM((GROUPS, count_tok, part), bf16),
            dma((3,)),
            dma((GROUPS,)),
            dma((GROUPS,)),
            dma((plane,)),
            dma((plane,)),
            dma((GROUPS,)),
            dma((GROUPS,)),
            dma((plane // 2, GROUPS)),
            dma((plane // 2, GROUPS)),
            dma((1,)),
            dma((1,)),
            dma((2, GROUPS)),
            dma((GROUPS,)),
            dma((GROUPS, plane)),
            dma((GROUPS, plane)),
            dma((GROUPS, plane, CHUNKS)),
            dma((GROUPS, plane, CHUNKS)),
            dma((GROUPS, CHUNKS)),
            dma((GROUPS, CHUNKS)),
        ],
        compiler_params=pltpu.CompilerParams(
            collective_id=0, has_side_effects=True, vmem_limit_bytes=60 * 1024 * 1024
        ),
    )(
        tokens, norm_gain.reshape(1, width), expert_ids.T, gate_weights.T,
        shared_gate, shared_up, shared_down.T, expert_gate, expert_up, expert_down,
    )


def solution(mesh):
    return jax.shard_map(
        per_device,
        mesh=mesh,
        in_specs=(
            P("ep", None),
            P(),
            P("ep", None),
            P("ep", None),
            P("ep", None, None),
            P("ep", None, None),
            P("ep", None, None),
            P("ep", None),
            P("ep", None),
            P(None, "ep"),
        ),
        out_specs=P("ep", None),
        check_vma=False,
    )
```

time: 155 us -> 103 us (0.66)
  Pallas kernels: 140 us -> 101 us
  other arithmetic: 8.65 us -> 0 us
  local copies, waits for them, and re-layouts: 4.97 us -> 1.88 us
    pallas_call x2 -> x1, Pallas kernels: 140 us -> 101 us  [per_device(): pl.pallas_call(functools.partial(moe_kernel, plane, slots, local), out_sh...]
    convert_element_type x4 -> x0, other arithmetic: 3.32 us -> none  [the longest x1 0.98 us: normalize(): return (scaled * norm_gain).astype(jnp.bfloat16)]
    reduce_sum x5 -> x0, other arithmetic: 3.19 us -> none  [the longest x1 1.13 us: per_device(): scale = jnp.sum(jnp.where(mine, weights, 0.0), axis=1)]
where the time goes in v1:
time: 103 us
  Pallas kernels  101 us (98%)
  local copies, waits for them, and re-layouts  1.88 us (2%)
    pallas_call x1, Pallas kernels, per_device(): pl.pallas_call(functools.partial(moe_kernel, plane, slots, local), out_sh...  101 us

profile of v1, /device:TPU:0, one launch (start us, length us, event | category | flops | bytes accessed | tf_op | source)
XLA Modules:
  0.0 102.8 jit_solution(12829223293807660883)
XLA Ops:
  0.0 101.0 %shard_map.100 = bf16[128,2048]{1,0:T(8,128)(2,1)} custom-call(bf16[128,2048]{1,0:T(8,128)(2,1)} %tok_ref.1, f32[1,2048]{1,0:T(1,128)} %bitcast.5, s32[4,128]{1,0:T(4,128)} %bitcast.6, f32[4,128]{1,0:T(4,128)} %bitcast.7, bf16[64,512]{1,0:T(8,128)(2,1)} %sgate_ref.1, bf16[64,512]{1,0:T(8,128)(2,1)} %sup_ref.1, bf16[64,512]{1,0:T(8,128)(2,1)} %bitcast.4, ...), custom_call_target="tpu_custom_call" | custom-call | tf_op jit(solution)/shard_map/pallas_call | solution.py:437
  101.0 1.9 %copy.12 = bf16[128,2048]{1,0:T(8,128)(2,1)} copy(bf16[128,2048]{1,0:T(8,128)(2,1)} %shard_map.100) | data formatting | bytes 1048576

commit v2 on v1

v2 whole, which is shorter than its diff:
```python
import functools

import jax
import jax.numpy as jnp
from jax import lax
from jax.experimental import pallas as pl
from jax.experimental.pallas import tpu as pltpu
from jax.sharding import PartitionSpec as P

EPS = 1e-06
GROUPS = 4
CHUNKS = 4
MESH = pl.DeviceIdType.MESH
ORDER = ((0, 1, 2, 3), (1, 2, 3, 0), (2, 1, 0, 3), (3, 2, 1, 0))
BACK = ((2, 3, 1), (3, 0, 2), (0, 3, 1), (1, 0, 2))
GOAL = ((1, 2, 1), (3, 0, 2), (0, 3, 1), (2, 1, 2))
SLOT = ((2, 3, 0), (1, 0, 1), (1, 0, 1), (2, 3, 0))


def pick(table, row, column):
    value = jnp.int32(table[0][column])
    for i in range(1, len(table)):
        value = jnp.where(row == i, jnp.int32(table[i][column]), value)
    return value


def stack_rows(rank, slots):
    slot = lax.broadcasted_iota(jnp.int32, (slots, rank.shape[1]), 0).astype(jnp.float32)
    return [rank[q : q + 1, :] == slot for q in range(rank.shape[0])]


def moe_kernel(
    plane, slots, local,
    tok_ref, gain_ref, ids_ref, wts_ref, sgate_ref, sup_ref, sdown_ref,
    gate_hbm, up_hbm, down_hbm,
    out_ref,
    gate, up, down, held, pack, packed, got, back, partial, land, route, slices, spread,
    w_sem, rsend, rrecv, fsend, frecv, hzsend, hzrecv, hpsend, hprecv, hcsend, hcrecv,
    zsend, zrecv, dsend, drecv, bsend, brecv, lsend, lrecv,
):
    f32, bf16 = jnp.float32, jnp.bfloat16
    me = lax.axis_index("ep")
    z, p = me // plane, me % plane
    chips, chip, core = plane // 2, p // 2, p % 2
    has_low, has_high = z > 0, z < GROUPS - 1
    middle = jnp.logical_and(has_low, has_high)
    outer = jnp.logical_not(middle)
    count_tok, width = tok_ref.shape
    top = ids_ref.shape[0]
    rows = plane * slots
    part = sgate_ref.shape[1] // GROUPS
    chunk = width // CHUNKS

    weights = [
        pltpu.make_async_copy(src, dst, w_sem.at[i])
        for i, (src, dst) in enumerate(((gate_hbm, gate), (up_hbm, up), (down_hbm, down)))
    ]
    for copy in weights:
        copy.start()

    barrier = pltpu.get_barrier_semaphore()

    def greet(device):
        pl.semaphore_signal(barrier, inc=1, device_id=(device,), device_id_type=MESH)

    for i in range(1, plane):
        greet(z * plane + (p + i) % plane)
    for j in range(1, GROUPS):
        greet((z + j) % GROUPS * plane + p)

    for g in range(GROUPS):
        for i, ref in enumerate((sgate_ref, sup_ref, sdown_ref)):
            slices[g, :, i * part : (i + 1) * part] = ref[:, g * part : (g + 1) * part]
    route[z, p, :top, :] = ids_ref[...].astype(f32)
    route[z, p, top:, :] = wts_ref[...]
    values = tok_ref[...].astype(f32)
    scaled = values * lax.rsqrt(jnp.mean(values * values, axis=-1, keepdims=True) + EPS)
    held[z] = (scaled * gain_ref[...]).astype(bf16)
    spread[z, chip, core] = slices[z]

    before = (
        lax.broadcasted_iota(jnp.int32, (count_tok, count_tok), 0)
        < lax.broadcasted_iota(jnp.int32, (count_tok, count_tok), 1)
    ).astype(bf16)

    def ranks(named):
        rank = jnp.dot(named.astype(bf16), before, preferred_element_type=f32)
        return jnp.where(named, rank, -1.0)

    def make_pack(g):
        first = (
            (lax.broadcasted_iota(jnp.int32, (plane, count_tok), 0) + z * plane) * local
        ).astype(f32)
        named = jnp.zeros((plane, count_tok), jnp.bool_)
        for k in range(top):
            ids = route[g, p, k : k + 1, :]
            named = jnp.logical_or(
                named, jnp.logical_and(ids >= first, ids < first + float(local))
            )
        blocks = stack_rows(ranks(named), slots)
        pack[g] = jnp.concatenate([b.astype(f32) for b in blocks], axis=0).astype(bf16)

    def fill(g, c):
        columns = pl.ds(c * chunk, chunk)
        packed[g, :, :, columns] = (
            jnp.dot(pack[g], held[g, :, columns], preferred_element_type=f32)
            .astype(bf16)
            .reshape(plane, slots, chunk)
        )

    make_pack(z)
    for c in range(CHUNKS):
        fill(z, c)
    pl.semaphore_wait(barrier, plane - 1 + GROUPS - 1)

    def total(sem, block):
        return pltpu.make_async_copy(block, block, sem).wait()

    others = pl.ds(0, plane - 1)

    def route_copy(j, g):
        return pltpu.make_async_remote_copy(
            src_ref=route.at[g, p], dst_ref=route.at[g, p],
            send_sem=rsend.at[0], recv_sem=rrecv.at[0],
            device_id=((z + j) % GROUPS * plane + p,), device_id_type=MESH,
        )

    def route_forward(i, q):
        return pltpu.make_async_remote_copy(
            src_ref=route.at[:, q], dst_ref=route.at[:, q],
            send_sem=fsend.at[0], recv_sem=frecv.at[0],
            device_id=(z * plane + (p + i) % plane,), device_id_type=MESH,
        )

    def slice_copy(j):
        g = (z + j) % GROUPS
        return pltpu.make_async_remote_copy(
            src_ref=slices.at[g], dst_ref=spread.at[z, chip, core],
            send_sem=hzsend.at[0], recv_sem=hzrecv.at[0],
            device_id=(g * plane + p,), device_id_type=MESH,
        )

    def column_copy(i, g, c):
        return pltpu.make_async_remote_copy(
            src_ref=spread.at[g, c, core], dst_ref=spread.at[g, c, core],
            send_sem=hpsend.at[0], recv_sem=hprecv.at[0],
            device_id=(z * plane + (chip + i) % chips * 2 + core,), device_id_type=MESH,
        )

    def core_copy(c):
        return pltpu.make_async_remote_copy(
            src_ref=spread.at[:, :, c], dst_ref=spread.at[:, :, c],
            send_sem=hcsend.at[0], recv_sem=hcrecv.at[0],
            device_id=(me + 1 - 2 * core,), device_id_type=MESH,
        )

    def along(g, c, direction):
        block = held.at[g, :, pl.ds(c * chunk, chunk)]
        return pltpu.make_async_remote_copy(
            src_ref=block, dst_ref=block,
            send_sem=zsend.at[direction, g], recv_sem=zrecv.at[g, c],
            device_id=(me + (plane if direction else -plane),), device_id_type=MESH,
        )

    def arrive_chunk(g, c):
        along(g, c, 0).wait_recv()

        @pl.when(jnp.logical_and(g > z, has_low))
        def _():
            along(g, c, 0).start()

        @pl.when(jnp.logical_and(g < z, has_high))
        def _():
            along(g, c, 1).start()

    def arrive(g):
        for c in range(CHUNKS):
            arrive_chunk(g, c)

    def dispatch_copy(g, q, c):
        columns = pl.ds(c * chunk, chunk)
        return pltpu.make_async_remote_copy(
            src_ref=packed.at[g, q, :, columns], dst_ref=got.at[g, p, :, columns],
            send_sem=dsend.at[0], recv_sem=drecv.at[g],
            device_id=(z * plane + q,), device_id_type=MESH,
        )

    def return_copy(g, q, c):
        columns = pl.ds(c * chunk, chunk)
        return pltpu.make_async_remote_copy(
            src_ref=got.at[g, q, :, columns], dst_ref=back.at[g, p, :, columns],
            send_sem=bsend.at[0], recv_sem=brecv.at[g, c],
            device_id=(z * plane + q,), device_id_type=MESH,
        )

    def dispatch(g, c):
        for i in range(1, plane):
            dispatch_copy(g, (p + i) % plane, c).start()
        columns = pl.ds(c * chunk, chunk)
        got[g, p, :, columns] = packed[g, p, :, columns]

    def give_back(g, c):
        for i in range(1, plane):
            return_copy(g, (p + i) % plane, c).start()

    def labels(g):
        came = jnp.zeros((plane, count_tok), jnp.bool_)
        which = jnp.zeros((plane, count_tok), f32)
        scale = jnp.zeros((plane, count_tok), f32)
        first = (me * local).astype(f32)
        for k in range(top):
            ids = route[g, :, k, :] - first
            mine = jnp.logical_and(ids >= 0.0, ids < float(local))
            came = jnp.logical_or(came, mine)
            which += jnp.where(mine, ids + 1.0, 0.0)
            scale += jnp.where(mine, route[g, :, top + k, :], 0.0)
        blocks = stack_rows(ranks(came), slots)
        label, weight = [], []
        for q, block in enumerate(blocks):
            label.append(
                jnp.sum(jnp.where(block, which[q : q + 1, :], 0.0), axis=1, keepdims=True)
            )
            weight.append(
                jnp.sum(jnp.where(block, scale[q : q + 1, :], 0.0), axis=1, keepdims=True)
            )
        return jnp.concatenate(label, axis=0) - 1.0, jnp.concatenate(weight, axis=0)

    def compute(g, send):
        label, weight = labels(g)
        total(drecv.at[g], got.at[g, others])
        x = got[g].reshape(rows, width)
        hidden = []
        for e in range(local):
            gate_val = jnp.dot(x, gate[e], preferred_element_type=f32)
            up_val = jnp.dot(x, up[e], preferred_element_type=f32)
            value = gate_val / (1.0 + jnp.exp(-gate_val)) * up_val
            hidden.append(jnp.where(label == float(e), value, 0.0).astype(bf16))
        for c in range(CHUNKS):
            columns = pl.ds(c * chunk, chunk)
            value = jnp.zeros((rows, chunk), f32)
            for e in range(local):
                value += jnp.dot(hidden[e], down[e, :, columns], preferred_element_type=f32)
            got[g, :, :, columns] = (value * weight).astype(bf16).reshape(plane, slots, chunk)
            if send:
                give_back(g, c)

        back[g, p] = got[g, p]

    def shared_hidden(g):
        pre = jnp.dot(
            held[g], spread[:, :, :, :, : 2 * part].reshape(width, 2 * part),
            preferred_element_type=f32,
        )
        gate_val, up_val = pre[:, :part], pre[:, part:]
        return (gate_val / (1.0 + jnp.exp(-gate_val)) * up_val).astype(bf16)

    def combined(g, c, hidden):
        columns = pl.ds(c * chunk, chunk)
        total(brecv.at[g, c], back.at[g, others, :, columns])
        value = lax.dot_general(
            pack[g], back[g, :, :, columns].reshape(rows, chunk), (((0,), (0,)), ((), ())),
            preferred_element_type=f32,
        )
        blocks = chunk // sgate_ref.shape[0]
        first = c * blocks
        down_t = spread[:, :, :, :, 2 * part :].reshape(width, part)[first * sgate_ref.shape[0] :][
            :chunk
        ]
        return value + lax.dot_general(
            hidden, down_t, (((1,), (1,)), ((), ())), preferred_element_type=f32
        )

    def land_copy(k, slot, goal, g, c):
        columns = pl.ds(c * chunk, chunk)
        return pltpu.make_async_remote_copy(
            src_ref=partial.at[g, :, columns], dst_ref=land.at[slot, :, columns],
            send_sem=lsend.at[0], recv_sem=lrecv.at[slot, c],
            device_id=(goal * plane + p,), device_id_type=MESH,
        )

    def pass_on(sums):
        hidden = [shared_hidden(pick(BACK, z, k)) for k, _ in sums]
        for c in range(CHUNKS):
            columns = pl.ds(c * chunk, chunk)
            for i, (k, joined) in enumerate(sums):
                g = pick(BACK, z, k)
                slot, goal = pick(SLOT, z, k), pick(GOAL, z, k)
                value = combined(g, c, hidden[i])
                if joined:
                    extra = GROUPS - k
                    land_copy(k, jnp.int32(extra), goal, g, c).wait_recv()
                    value += land[extra, :, columns].astype(f32)
                partial[g, :, columns] = value.astype(bf16)
                land_copy(k, slot, goal, g, c).start()

    for j in range(1, GROUPS):
        route_copy(j, z).start()
    for c in range(CHUNKS):

        @pl.when(has_low)
        def _():
            along(z, c, 0).start()

        @pl.when(has_high)
        def _():
            along(z, c, 1).start()

    for j in range(1, GROUPS):
        slice_copy(j).start()
    for i in range(1, chips):
        column_copy(i, z, chip).start()
    for c in range(CHUNKS):
        dispatch(z, c)
    total(rrecv.at[0], route.at[pl.ds(0, GROUPS - 1), p])
    for i in range(1, plane):
        route_forward(i, p).start()
    for j in range(1, GROUPS):
        make_pack((z + j) % GROUPS)

    one, two, three = (pick(ORDER, z, k) for k in range(1, GROUPS))
    for c in range(CHUNKS):
        arrive_chunk(one, c)

        @pl.when(middle)
        def _():
            arrive_chunk(three, c)

        fill(one, c)
        dispatch(one, c)

    total(hzrecv.at[0], spread.at[pl.ds(0, GROUPS - 1), chip, core])
    for i in range(1, chips):
        for j in range(1, GROUPS):
            column_copy(i, (z + j) % GROUPS, chip).start()
    total(frecv.at[0], route.at[:, others])
    for copy in weights:
        copy.wait()
    compute(z, False)
    for c in range(CHUNKS):
        arrive_chunk(two, c)
        fill(two, c)
        dispatch(two, c)
    compute(one, False)
    total(hprecv.at[0], spread.at[:, pl.ds(0, chips - 1), core])
    core_copy(core).start()
    for c in range(CHUNKS):

        @pl.when(outer)
        def _():
            arrive_chunk(three, c)

        fill(three, c)
        dispatch(three, c)

    compute(two, True)
    compute(three, True)
    for c in range(CHUNKS):
        give_back(one, c)
    for c in range(CHUNKS):
        give_back(z, c)
    core_copy(1 - core).wait_recv()
    pass_on(((0, False),))

    @pl.when(outer)
    def _():
        pass_on(((1, False),))
        pass_on(((2, False),))

    @pl.when(middle)
    def _():
        pass_on(((1, True), (2, True)))

    hidden = shared_hidden(z)
    for c in range(CHUNKS):
        columns = pl.ds(c * chunk, chunk)
        value = combined(z, c, hidden)
        for slot in range(2):
            land_copy(0, jnp.int32(slot), z, z, c).wait_recv()
            value += land[slot, :, columns].astype(f32)
        out_ref[:, columns] = value.astype(out_ref.dtype)

    total(rsend.at[0], route.at[pl.ds(0, GROUPS - 1), p])
    total(hzsend.at[0], slices.at[pl.ds(0, GROUPS - 1)])
    total(fsend.at[0], route.at[:, others])
    total(hpsend.at[0], spread.at[:, pl.ds(0, chips - 1), core])
    core_copy(core).wait_send()
    total(dsend.at[0], packed.at[:, others])
    total(bsend.at[0], got.at[:, others])
    total(lsend.at[0], partial.at[pl.ds(0, GROUPS - 1)])
    for g in range(GROUPS):

        @pl.when(jnp.logical_and(g >= z, has_low))
        def _():
            total(zsend.at[0, g], held.at[g])

        @pl.when(jnp.logical_and(g <= z, has_high))
        def _():
            total(zsend.at[1, g], held.at[g])


def per_device(
    tokens, norm_gain, expert_ids, gate_weights, expert_gate, expert_up, expert_down,
    shared_gate, shared_up, shared_down,
):
    bf16, f32 = jnp.bfloat16, jnp.float32
    count_tok, width = tokens.shape
    top = expert_ids.shape[1]
    local = expert_gate.shape[0]
    devices = lax.axis_size("ep")
    plane = devices // GROUPS
    mean_rows = count_tok * top // devices
    capacity = mean_rows + mean_rows // 2
    slots = -(-capacity // 8) * 8
    rows = plane * slots
    depth, hidden = shared_gate.shape
    part = hidden // GROUPS
    dma = pltpu.SemaphoreType.DMA
    vmem = pl.BlockSpec(memory_space=pltpu.VMEM)
    hbm = pl.BlockSpec(memory_space=pl.ANY)
    blocks = (GROUPS, plane, slots, width)
    whole = (GROUPS, count_tok, width)
    return pl.pallas_call(
        functools.partial(moe_kernel, plane, slots, local),
        out_shape=jax.ShapeDtypeStruct((count_tok, width), bf16),
        in_specs=[vmem] * 7 + [hbm] * 3,
        out_specs=vmem,
        scratch_shapes=[
            pltpu.VMEM(expert_gate.shape, bf16),
            pltpu.VMEM(expert_up.shape, bf16),
            pltpu.VMEM(expert_down.shape, bf16),
            pltpu.VMEM(whole, bf16),
            pltpu.VMEM((GROUPS, rows, count_tok), bf16),
            pltpu.VMEM(blocks, bf16),
            pltpu.VMEM(blocks, bf16),
            pltpu.VMEM(blocks, bf16),
            pltpu.VMEM(whole, bf16),
            pltpu.VMEM(whole, bf16),
            pltpu.VMEM((GROUPS, plane, 2 * top, count_tok), f32),
            pltpu.VMEM((GROUPS, depth, 3 * part), bf16),
            pltpu.VMEM((GROUPS, plane // 2, 2, depth, 3 * part), bf16),
            dma((3,)),
            dma((1,)),
            dma((1,)),
            dma((1,)),
            dma((1,)),
            dma((1,)),
            dma((1,)),
            dma((1,)),
            dma((1,)),
            dma((1,)),
            dma((1,)),
            dma((2, GROUPS)),
            dma((GROUPS, CHUNKS)),
            dma((1,)),
            dma((GROUPS,)),
            dma((1,)),
            dma((GROUPS, CHUNKS)),
            dma((1,)),
            dma((GROUPS, CHUNKS)),
        ],
        compiler_params=pltpu.CompilerParams(
            collective_id=0, has_side_effects=True, vmem_limit_bytes=60 * 1024 * 1024
        ),
    )(
        tokens, norm_gain.reshape(1, width), expert_ids.T, gate_weights.T,
        shared_gate, shared_up, shared_down.T, expert_gate, expert_up, expert_down,
    )


def solution(mesh):
    return jax.shard_map(
        per_device,
        mesh=mesh,
        in_specs=(
            P("ep", None),
            P(),
            P("ep", None),
            P("ep", None),
            P("ep", None, None),
            P("ep", None, None),
            P("ep", None, None),
            P("ep", None),
            P("ep", None),
            P(None, "ep"),
        ),
        out_specs=P("ep", None),
        check_vma=False,
    )
```

time: 103 us -> 94.8 us (0.920)
  Pallas kernels: 101 us -> 92.8 us
    pallas_call x1, Pallas kernels: 101 us -> 92.8 us  [per_device(): pl.pallas_call(functools.partial(moe_kernel, plane, slots, local), out_sh...]
where the time goes in v2:
time: 94.8 us; the launch traced here: 94.7 us
  Pallas kernels  92.8 us (98%)
  local copies, waits for them, and re-layouts  1.88 us (2%)
    pallas_call x1, Pallas kernels, per_device(): pl.pallas_call(functools.partial(moe_kernel, plane, slots, local), out_sh...  92.8 us

profile of v2, /device:TPU:0, one launch (start us, length us, event | category | flops | bytes accessed | tf_op | source)
XLA Modules:
  0.0 94.7 jit_solution(1997527939454983233)
XLA Ops:
  0.0 92.8 %shard_map.100 = bf16[128,2048]{1,0:T(8,128)(2,1)} custom-call(bf16[128,2048]{1,0:T(8,128)(2,1)} %tok_ref.1, f32[1,2048]{1,0:T(1,128)} %bitcast.5, s32[4,128]{1,0:T(4,128)} %bitcast.6, f32[4,128]{1,0:T(4,128)} %bitcast.7, bf16[64,512]{1,0:T(8,128)(2,1)} %sgate_ref.1, bf16[64,512]{1,0:T(8,128)(2,1)} %sup_ref.1, bf16[64,512]{1,0:T(8,128)(2,1)} %bitcast.4, ...), custom_call_target="tpu_custom_call" | custom-call | tf_op jit(solution)/shard_map/pallas_call | solution.py:422
  92.8 1.9 %copy.12 = bf16[128,2048]{1,0:T(8,128)(2,1)} copy(bf16[128,2048]{1,0:T(8,128)(2,1)} %shard_map.100) | data formatting | bytes 1048576

commit v3 on v2

--- a/solution.py
+++ b/solution.py
@@ -10,11 +10,12 @@
 EPS = 1e-06
 GROUPS = 4
 CHUNKS = 4
+EARLY = 2
 MESH = pl.DeviceIdType.MESH
 ORDER = ((0, 1, 2, 3), (1, 2, 3, 0), (2, 1, 0, 3), (3, 2, 1, 0))
-BACK = ((2, 3, 1), (3, 0, 2), (0, 3, 1), (1, 0, 2))
-GOAL = ((1, 2, 1), (3, 0, 2), (0, 3, 1), (2, 1, 2))
-SLOT = ((2, 3, 0), (1, 0, 1), (1, 0, 1), (2, 3, 0))
+BACK = ((1, 2, 3), (3, 2, 0), (0, 1, 3), (2, 1, 0))
+GOAL = ((1, 1, 2), (3, 2, 0), (0, 1, 3), (2, 2, 1))
+SLOT = ((0, 2, 3), (1, 1, 0), (1, 1, 0), (0, 2, 3))
 
 
 def pick(table, row, column):
@@ -34,7 +35,7 @@
     tok_ref, gain_ref, ids_ref, wts_ref, sgate_ref, sup_ref, sdown_ref,
     gate_hbm, up_hbm, down_hbm,
     out_ref,
-    gate, up, down, held, pack, packed, got, back, partial, land, route, slices, spread,
+    gate, up, down, held, pack, packed, got, back, partial, land, route, slices, spread, hidden_s,
     w_sem, rsend, rrecv, fsend, frecv, hzsend, hzrecv, hpsend, hprecv, hcsend, hcrecv,
     zsend, zrecv, dsend, drecv, bsend, brecv, lsend, lrecv,
 ):
@@ -140,12 +141,16 @@
             device_id=(g * plane + p,), device_id_type=MESH,
         )
 
-    def column_copy(i, g, c):
+    def column_copy(goal, g, c, sem):
         return pltpu.make_async_remote_copy(
             src_ref=spread.at[g, c, core], dst_ref=spread.at[g, c, core],
-            send_sem=hpsend.at[0], recv_sem=hprecv.at[0],
-            device_id=(z * plane + (chip + i) % chips * 2 + core,), device_id_type=MESH,
-        )
+            send_sem=hpsend.at[0], recv_sem=hprecv.at[sem],
+            device_id=(z * plane + goal * 2 + core,), device_id_type=MESH,
+        )
+
+    square = chips == 4
+    beside, across = chip + 1 - 2 * (chip % 2), (chip + 2) % chips
+    near = (beside, across) if square else [(chip + i) % chips for i in range(1, chips)]
 
     def core_copy(c):
         return pltpu.make_async_remote_copy(
@@ -225,7 +230,7 @@
             )
         return jnp.concatenate(label, axis=0) - 1.0, jnp.concatenate(weight, axis=0)
 
-    def compute(g, send):
+    def compute(g, send, midway=None):
         label, weight = labels(g)
         total(drecv.at[g], got.at[g, others])
         x = got[g].reshape(rows, width)
@@ -243,6 +248,8 @@
             got[g, :, :, columns] = (value * weight).astype(bf16).reshape(plane, slots, chunk)
             if send:
                 give_back(g, c)
+            if midway is not None and c == EARLY - 1:
+                midway()
 
         back[g, p] = got[g, p]
 
@@ -252,9 +259,9 @@
             preferred_element_type=f32,
         )
         gate_val, up_val = pre[:, :part], pre[:, part:]
-        return (gate_val / (1.0 + jnp.exp(-gate_val)) * up_val).astype(bf16)
-
-    def combined(g, c, hidden):
+        hidden_s[g] = (gate_val / (1.0 + jnp.exp(-gate_val)) * up_val).astype(bf16)
+
+    def combined(g, c):
         columns = pl.ds(c * chunk, chunk)
         total(brecv.at[g, c], back.at[g, others, :, columns])
         value = lax.dot_general(
@@ -267,7 +274,7 @@
             :chunk
         ]
         return value + lax.dot_general(
-            hidden, down_t, (((1,), (1,)), ((), ())), preferred_element_type=f32
+            hidden_s[g], down_t, (((1,), (1,)), ((), ())), preferred_element_type=f32
         )
 
     def land_copy(k, slot, goal, g, c):
@@ -278,20 +285,17 @@
             device_id=(goal * plane + p,), device_id_type=MESH,
         )
 
-    def pass_on(sums):
-        hidden = [shared_hidden(pick(BACK, z, k)) for k, _ in sums]
-        for c in range(CHUNKS):
-            columns = pl.ds(c * chunk, chunk)
-            for i, (k, joined) in enumerate(sums):
-                g = pick(BACK, z, k)
-                slot, goal = pick(SLOT, z, k), pick(GOAL, z, k)
-                value = combined(g, c, hidden[i])
-                if joined:
-                    extra = GROUPS - k
-                    land_copy(k, jnp.int32(extra), goal, g, c).wait_recv()
-                    value += land[extra, :, columns].astype(f32)
-                partial[g, :, columns] = value.astype(bf16)
-                land_copy(k, slot, goal, g, c).start()
+    def pass_on(k, c, joined=False):
+        g = pick(BACK, z, k)
+        columns = pl.ds(c * chunk, chunk)
+        slot, goal = pick(SLOT, z, k), pick(GOAL, z, k)
+        value = combined(g, c)
+        if joined:
+            extra = k + 1
+            land_copy(k, jnp.int32(extra), goal, g, c).wait_recv()
+            value += land[extra, :, columns].astype(f32)
+        partial[g, :, columns] = value.astype(bf16)
+        land_copy(k, slot, goal, g, c).start()
 
     for j in range(1, GROUPS):
         route_copy(j, z).start()
@@ -307,8 +311,8 @@
 
     for j in range(1, GROUPS):
         slice_copy(j).start()
-    for i in range(1, chips):
-        column_copy(i, z, chip).start()
+    for goal in near:
+        column_copy(goal, z, chip, 0).start()
     for c in range(CHUNKS):
         dispatch(z, c)
     total(rrecv.at[0], route.at[pl.ds(0, GROUPS - 1), p])
@@ -329,51 +333,133 @@
         dispatch(one, c)
 
     total(hzrecv.at[0], spread.at[pl.ds(0, GROUPS - 1), chip, core])
-    for i in range(1, chips):
+    for goal in near:
         for j in range(1, GROUPS):
-            column_copy(i, (z + j) % GROUPS, chip).start()
+            column_copy(goal, (z + j) % GROUPS, chip, 0).start()
     total(frecv.at[0], route.at[:, others])
     for copy in weights:
         copy.wait()
     compute(z, False)
+
+    def hand_over():
+        total(hprecv.at[0], spread.at[:, pl.ds(0, len(near)), core])
+        if square:
+            for g in range(GROUPS // 2):
+                column_copy(across, g, beside, 1).start()
+            for g in range(GROUPS // 2, GROUPS):
+                column_copy(beside, g, across, 1).start()
+
+    def share():
+        if square:
+            total(hprecv.at[1], spread.at[:, 0, core])
+        core_copy(core).start()
+
     for c in range(CHUNKS):
         arrive_chunk(two, c)
         fill(two, c)
         dispatch(two, c)
+        if c == 1:
+
+            @pl.when(middle)
+            def _():
+                hand_over()
+
+    @pl.when(outer)
+    def _():
+        hand_over()
+
     compute(one, False)
-    total(hprecv.at[0], spread.at[:, pl.ds(0, chips - 1), core])
-    core_copy(core).start()
-    for c in range(CHUNKS):
-
+
+    @pl.when(outer)
+    def _():
+        for c in range(EARLY):
+            give_back(one, c)
+        for c in range(EARLY):
+            arrive_chunk(three, c)
+            fill(three, c)
+            dispatch(three, c)
+        share()
+
+    @pl.when(middle)
+    def _():
+        fill(three, 0)
+        dispatch(three, 0)
+
+    def rest_of_three():
         @pl.when(outer)
         def _():
-            arrive_chunk(three, c)
-
-        fill(three, c)
-        dispatch(three, c)
-
-    compute(two, True)
-    compute(three, True)
-    for c in range(CHUNKS):
-        give_back(one, c)
+            for c in range(EARLY, CHUNKS):
+                arrive_chunk(three, c)
+                fill(three, c)
+                dispatch(three, c)
+
+    compute(two, True, rest_of_three)
+
+    @pl.when(outer)
+    def _():
+        core_copy(1 - core).wait_recv()
+        shared_hidden(one)
+        for c in range(EARLY):
+            pass_on(0, c)
+        shared_hidden(two)
+        for c in range(EARLY):
+            pass_on(1, c)
+
+    @pl.when(middle)
+    def _():
+        for c in range(EARLY):
+            give_back(one, c)
+        for c in range(1, CHUNKS):
+            fill(three, c)
+            dispatch(three, c)
+        for c in range(EARLY, CHUNKS):
+            give_back(one, c)
+        share()
+        core_copy(1 - core).wait_recv()
+        shared_hidden(two)
+        for c in range(CHUNKS):
+            pass_on(0, c)
+        shared_hidden(one)
+        for c in range(EARLY):
+            pass_on(1, c, True)
+
+    def third_of_two():
+        @pl.when(outer)
+        def _():
+            pass_on(1, EARLY)
+
+    compute(three, True, third_of_two)
+
+    @pl.when(outer)
+    def _():
+        for c in range(EARLY, CHUNKS):
+            give_back(one, c)
+
     for c in range(CHUNKS):
         give_back(z, c)
-    core_copy(1 - core).wait_recv()
-    pass_on(((0, False),))
 
     @pl.when(outer)
     def _():
-        pass_on(((1, False),))
-        pass_on(((2, False),))
+        shared_hidden(three)
+        for c in range(EARLY + 1, CHUNKS):
+            pass_on(1, c)
+        for c in range(CHUNKS):
+            pass_on(2, c)
+        for c in range(EARLY, CHUNKS):
+            pass_on(0, c)
 
     @pl.when(middle)
     def _():
-        pass_on(((1, True), (2, True)))
-
-    hidden = shared_hidden(z)
-    for c in range(CHUNKS):
-        columns = pl.ds(c * chunk, chunk)
-        value = combined(z, c, hidden)
+        shared_hidden(three)
+        for c in range(EARLY, CHUNKS):
+            pass_on(1, c, True)
+        for c in range(CHUNKS):
+            pass_on(2, c, True)
+
+    shared_hidden(z)
+    for c in range(CHUNKS):
+        columns = pl.ds(c * chunk, chunk)
+        value = combined(z, c)
         for slot in range(2):
             land_copy(0, jnp.int32(slot), z, z, c).wait_recv()
             value += land[slot, :, columns].astype(f32)
@@ -438,6 +524,7 @@
             pltpu.VMEM((GROUPS, plane, 2 * top, count_tok), f32),
             pltpu.VMEM((GROUPS, depth, 3 * part), bf16),
             pltpu.VMEM((GROUPS, plane // 2, 2, depth, 3 * part), bf16),
+            pltpu.VMEM((GROUPS, count_tok, part), bf16),
             dma((3,)),
             dma((1,)),
             dma((1,)),
@@ -446,7 +533,7 @@
             dma((1,)),
             dma((1,)),
             dma((1,)),
-            dma((1,)),
+            dma((2,)),
             dma((1,)),
             dma((1,)),
             dma((2, GROUPS)),

time: 94.8 us -> 89.8 us (0.947)
  Pallas kernels: 92.8 us -> 87.7 us
    pallas_call x1, Pallas kernels: 92.8 us -> 87.7 us  [per_device(): pl.pallas_call(functools.partial(moe_kernel, plane, slots, local), out_sh...]
where the time goes in v3:
time: 89.8 us; the launch traced here: 89.6 us
  Pallas kernels  87.7 us (98%)
  local copies, waits for them, and re-layouts  1.88 us (2%)
    pallas_call x1, Pallas kernels, per_device(): pl.pallas_call(functools.partial(moe_kernel, plane, slots, local), out_sh...  87.7 us
    unnamed x1, local copies, waits for them, and re-layouts  1.88 us

profile of v3, /device:TPU:0, one launch (start us, length us, event | category | flops | bytes accessed | tf_op | source)
XLA Modules:
  0.0 89.6 jit_solution(13004542988988643760)
XLA Ops:
  0.0 87.7 %shard_map.100 = bf16[128,2048]{1,0:T(8,128)(2,1)} custom-call(bf16[128,2048]{1,0:T(8,128)(2,1)} %tok_ref.1, f32[1,2048]{1,0:T(1,128)} %bitcast.5, s32[4,128]{1,0:T(4,128)} %bitcast.6, f32[4,128]{1,0:T(4,128)} %bitcast.7, bf16[64,512]{1,0:T(8,128)(2,1)} %sgate_ref.1, bf16[64,512]{1,0:T(8,128)(2,1)} %sup_ref.1, bf16[64,512]{1,0:T(8,128)(2,1)} %bitcast.4, ...), custom_call_target="tpu_custom_call" | custom-call | tf_op jit(solution)/shard_map/pallas_call | solution.py:508
  87.8 1.9 %copy.12 = bf16[128,2048]{1,0:T(8,128)(2,1)} copy(bf16[128,2048]{1,0:T(8,128)(2,1)} %shard_map.100) | data formatting | bytes 1048576

commit v4 on v3

--- a/solution.py
+++ b/solution.py
@@ -32,9 +32,10 @@
 
 def moe_kernel(
     plane, slots, local,
-    tok_ref, gain_ref, ids_ref, wts_ref, sgate_ref, sup_ref, sdown_ref,
+    tok_hbm, gain_hbm, ids_hbm, wts_hbm, sgate_hbm, sup_hbm, sdown_hbm,
     gate_hbm, up_hbm, down_hbm,
     out_ref,
+    tok_ref, gain_ref, ids_ref, wts_ref, sgate_ref, sup_ref, sdown_ref, in_sem,
     gate, up, down, held, pack, packed, got, back, partial, land, route, slices, spread, hidden_s,
     w_sem, rsend, rrecv, fsend, frecv, hzsend, hzrecv, hpsend, hprecv, hcsend, hcrecv,
     zsend, zrecv, dsend, drecv, bsend, brecv, lsend, lrecv,
@@ -52,6 +53,28 @@
     part = sgate_ref.shape[1] // GROUPS
     chunk = width // CHUNKS
 
+    inputs = [
+        pltpu.make_async_copy(src, dst, in_sem.at[i])
+        for i, (src, dst) in enumerate(
+            (
+                (tok_hbm, tok_ref), (gain_hbm, gain_ref), (ids_hbm, ids_ref),
+                (wts_hbm, wts_ref), (sgate_hbm, sgate_ref), (sup_hbm, sup_ref),
+                (sdown_hbm, sdown_ref),
+            )
+        )
+    ]
+    for copy in inputs:
+        copy.start()
+    barrier = pltpu.get_barrier_semaphore()
+
+    def greet(device):
+        pl.semaphore_signal(barrier, inc=1, device_id=(device,), device_id_type=MESH)
+
+    for i in range(1, plane):
+        greet(z * plane + (p + i) % plane)
+    for j in range(1, GROUPS):
+        greet((z + j) % GROUPS * plane + p)
+
     weights = [
         pltpu.make_async_copy(src, dst, w_sem.at[i])
         for i, (src, dst) in enumerate(((gate_hbm, gate), (up_hbm, up), (down_hbm, down)))
@@ -59,16 +82,8 @@
     for copy in weights:
         copy.start()
 
-    barrier = pltpu.get_barrier_semaphore()
-
-    def greet(device):
-        pl.semaphore_signal(barrier, inc=1, device_id=(device,), device_id_type=MESH)
-
-    for i in range(1, plane):
-        greet(z * plane + (p + i) % plane)
-    for j in range(1, GROUPS):
-        greet((z + j) % GROUPS * plane + p)
-
+    for copy in inputs:
+        copy.wait()
     for g in range(GROUPS):
         for i, ref in enumerate((sgate_ref, sup_ref, sdown_ref)):
             slices[g, :, i * part : (i + 1) * part] = ref[:, g * part : (g + 1) * part]
@@ -109,9 +124,6 @@
             .reshape(plane, slots, chunk)
         )
 
-    make_pack(z)
-    for c in range(CHUNKS):
-        fill(z, c)
     pl.semaphore_wait(barrier, plane - 1 + GROUPS - 1)
 
     def total(sem, block):
@@ -313,7 +325,9 @@
         slice_copy(j).start()
     for goal in near:
         column_copy(goal, z, chip, 0).start()
+    make_pack(z)
     for c in range(CHUNKS):
+        fill(z, c)
         dispatch(z, c)
     total(rrecv.at[0], route.at[pl.ds(0, GROUPS - 1), p])
     for i in range(1, plane):
@@ -501,16 +515,23 @@
     depth, hidden = shared_gate.shape
     part = hidden // GROUPS
     dma = pltpu.SemaphoreType.DMA
-    vmem = pl.BlockSpec(memory_space=pltpu.VMEM)
-    hbm = pl.BlockSpec(memory_space=pl.ANY)
+    hbm = pl.BlockSpec(memory_space=pltpu.HBM)
     blocks = (GROUPS, plane, slots, width)
     whole = (GROUPS, count_tok, width)
     return pl.pallas_call(
         functools.partial(moe_kernel, plane, slots, local),
         out_shape=jax.ShapeDtypeStruct((count_tok, width), bf16),
-        in_specs=[vmem] * 7 + [hbm] * 3,
-        out_specs=vmem,
+        in_specs=[hbm] * 10,
+        out_specs=pl.BlockSpec(memory_space=pltpu.VMEM),
         scratch_shapes=[
+            pltpu.VMEM(tokens.shape, bf16),
+            pltpu.VMEM((1, width), f32),
+            pltpu.VMEM((top, count_tok), jnp.int32),
+            pltpu.VMEM((top, count_tok), f32),
+            pltpu.VMEM(shared_gate.shape, bf16),
+            pltpu.VMEM(shared_gate.shape, bf16),
+            pltpu.VMEM(shared_gate.shape, bf16),
+            dma((7,)),
             pltpu.VMEM(expert_gate.shape, bf16),
             pltpu.VMEM(expert_up.shape, bf16),
             pltpu.VMEM(expert_down.shape, bf16),
@@ -546,11 +567,16 @@
             dma((GROUPS, CHUNKS)),
         ],
         compiler_params=pltpu.CompilerParams(
-            collective_id=0, has_side_effects=True, vmem_limit_bytes=60 * 1024 * 1024
+            collective_id=0, has_side_effects=True, vmem_limit_bytes=52 * 1024 * 1024
         ),
     )(
-        tokens, norm_gain.reshape(1, width), expert_ids.T, gate_weights.T,
-        shared_gate, shared_up, shared_down.T, expert_gate, expert_up, expert_down,
+        *[
+            pltpu.with_memory_space_constraint(x, pltpu.HBM)
+            for x in (
+                tokens, norm_gain.reshape(1, width), expert_ids.T, gate_weights.T,
+                shared_gate, shared_up, shared_down.T, expert_gate, expert_up, expert_down,
+            )
+        ]
     )
 
 

time: 89.8 us -> 86.3 us (0.961)
  Pallas kernels: 87.7 us -> 85.4 us
  local copies, waits for them, and re-layouts: 1.88 us -> 0.8 us
    pallas_call x1, Pallas kernels: 87.7 us -> 85.4 us  [per_device(): pl.pallas_call(functools.partial(moe_kernel, plane, slots, local), out_sh...]
    unnamed x1, local copies, waits for them, and re-layouts: 1.88 us -> 0.8 us
where the time goes in v4:
time: 86.3 us; the launch traced here: 86.2 us
  Pallas kernels  85.4 us (99%)
    pallas_call x1, Pallas kernels, per_device(): pl.pallas_call(functools.partial(moe_kernel, plane, slots, local), out_sh...  85.4 us

profile of v4, /device:TPU:0, one launch (start us, length us, event | category | flops | bytes accessed | tf_op | source)
XLA Modules:
  0.0 86.2 jit_solution(2131987330985371038)
XLA Ops:
  0.0 85.4 %shard_map.100 = bf16[128,2048]{1,0:T(8,128)(2,1)S(1)} custom-call(bf16[128,2048]{1,0:T(8,128)(2,1)} %tok_hbm.1, f32[1,2048]{1,0:T(1,128)} %bitcast.5, s32[4,128]{1,0:T(4,128)} %bitcast.6, f32[4,128]{1,0:T(4,128)} %bitcast.7, bf16[64,512]{1,0:T(8,128)(2,1)} %sgate_hbm.1, bf16[64,512]{1,0:T(8,128)(2,1)} %sup_hbm.1, bf16[64,512]{1,0:T(8,128)(2,1)} %bitcast.4, ...), custom_call_target="tpu_custom_call" | custom-call | tf_op jit(solution)/shard_map/pallas_call | solution.py:521
  85.4 0.8 copy.12

commit v5 on v4

--- a/solution.py
+++ b/solution.py
@@ -11,6 +11,7 @@
 GROUPS = 4
 CHUNKS = 4
 EARLY = 2
+HALVES = 2
 MESH = pl.DeviceIdType.MESH
 ORDER = ((0, 1, 2, 3), (1, 2, 3, 0), (2, 1, 0, 3), (3, 2, 1, 0))
 BACK = ((1, 2, 3), (3, 2, 0), (0, 1, 3), (2, 1, 0))
@@ -36,7 +37,7 @@
     gate_hbm, up_hbm, down_hbm,
     out_ref,
     tok_ref, gain_ref, ids_ref, wts_ref, sgate_ref, sup_ref, sdown_ref, in_sem,
-    gate, up, down, held, pack, packed, got, back, partial, land, route, slices, spread, hidden_s,
+    gate, up, down, held, pack, unpack, packed, got, back, partial, land, route, share_of, slices, spread, hidden_s,
     w_sem, rsend, rrecv, fsend, frecv, hzsend, hzrecv, hpsend, hprecv, hcsend, hcrecv,
     zsend, zrecv, dsend, drecv, bsend, brecv, lsend, lrecv,
 ):
@@ -52,6 +53,7 @@
     rows = plane * slots
     part = sgate_ref.shape[1] // GROUPS
     chunk = width // CHUNKS
+    piece = chunk // HALVES
 
     inputs = [
         pltpu.make_async_copy(src, dst, in_sem.at[i])
@@ -87,8 +89,8 @@
     for g in range(GROUPS):
         for i, ref in enumerate((sgate_ref, sup_ref, sdown_ref)):
             slices[g, :, i * part : (i + 1) * part] = ref[:, g * part : (g + 1) * part]
-    route[z, p, :top, :] = ids_ref[...].astype(f32)
-    route[z, p, top:, :] = wts_ref[...]
+    route[p, z] = ids_ref[...].astype(f32)
+    share_of[z] = wts_ref[...]
     values = tok_ref[...].astype(f32)
     scaled = values * lax.rsqrt(jnp.mean(values * values, axis=-1, keepdims=True) + EPS)
     held[z] = (scaled * gain_ref[...]).astype(bf16)
@@ -108,13 +110,20 @@
             (lax.broadcasted_iota(jnp.int32, (plane, count_tok), 0) + z * plane) * local
         ).astype(f32)
         named = jnp.zeros((plane, count_tok), jnp.bool_)
+        scale = jnp.zeros((plane, count_tok), f32)
         for k in range(top):
-            ids = route[g, p, k : k + 1, :]
-            named = jnp.logical_or(
-                named, jnp.logical_and(ids >= first, ids < first + float(local))
-            )
+            ids = route[p, g, k : k + 1, :]
+            here = jnp.logical_and(ids >= first, ids < first + float(local))
+            named = jnp.logical_or(named, here)
+            scale += jnp.where(here, share_of[g, k : k + 1, :], 0.0)
         blocks = stack_rows(ranks(named), slots)
         pack[g] = jnp.concatenate([b.astype(f32) for b in blocks], axis=0).astype(bf16)
+        weighted = jnp.concatenate(
+            [jnp.where(b, scale[q : q + 1, :], 0.0) for q, b in enumerate(blocks)], axis=0
+        )
+        upper = weighted.astype(bf16)
+        unpack[g, 0] = upper
+        unpack[g, 1] = (weighted - upper.astype(f32)).astype(bf16)
 
     def fill(g, c):
         columns = pl.ds(c * chunk, chunk)
@@ -131,16 +140,16 @@
 
     others = pl.ds(0, plane - 1)
 
-    def route_copy(j, g):
-        return pltpu.make_async_remote_copy(
-            src_ref=route.at[g, p], dst_ref=route.at[g, p],
-            send_sem=rsend.at[0], recv_sem=rrecv.at[0],
+    def route_copy(j, ref, sem):
+        return pltpu.make_async_remote_copy(
+            src_ref=ref, dst_ref=ref,
+            send_sem=rsend.at[sem], recv_sem=rrecv.at[sem],
             device_id=((z + j) % GROUPS * plane + p,), device_id_type=MESH,
         )
 
     def route_forward(i, q):
         return pltpu.make_async_remote_copy(
-            src_ref=route.at[:, q], dst_ref=route.at[:, q],
+            src_ref=route.at[q], dst_ref=route.at[q],
             send_sem=fsend.at[0], recv_sem=frecv.at[0],
             device_id=(z * plane + (p + i) % plane,), device_id_type=MESH,
         )
@@ -223,27 +232,21 @@
     def labels(g):
         came = jnp.zeros((plane, count_tok), jnp.bool_)
         which = jnp.zeros((plane, count_tok), f32)
-        scale = jnp.zeros((plane, count_tok), f32)
         first = (me * local).astype(f32)
         for k in range(top):
-            ids = route[g, :, k, :] - first
+            ids = route[:, g, k, :] - first
             mine = jnp.logical_and(ids >= 0.0, ids < float(local))
             came = jnp.logical_or(came, mine)
             which += jnp.where(mine, ids + 1.0, 0.0)
-            scale += jnp.where(mine, route[g, :, top + k, :], 0.0)
         blocks = stack_rows(ranks(came), slots)
-        label, weight = [], []
-        for q, block in enumerate(blocks):
-            label.append(
-                jnp.sum(jnp.where(block, which[q : q + 1, :], 0.0), axis=1, keepdims=True)
-            )
-            weight.append(
-                jnp.sum(jnp.where(block, scale[q : q + 1, :], 0.0), axis=1, keepdims=True)
-            )
-        return jnp.concatenate(label, axis=0) - 1.0, jnp.concatenate(weight, axis=0)
+        label = [
+            jnp.sum(jnp.where(block, which[q : q + 1, :], 0.0), axis=1, keepdims=True)
+            for q, block in enumerate(blocks)
+        ]
+        return jnp.concatenate(label, axis=0) - 1.0
 
     def compute(g, send, midway=None):
-        label, weight = labels(g)
+        label = labels(g)
         total(drecv.at[g], got.at[g, others])
         x = got[g].reshape(rows, width)
         hidden = []
@@ -257,7 +260,7 @@
             value = jnp.zeros((rows, chunk), f32)
             for e in range(local):
                 value += jnp.dot(hidden[e], down[e, :, columns], preferred_element_type=f32)
-            got[g, :, :, columns] = (value * weight).astype(bf16).reshape(plane, slots, chunk)
+            got[g, :, :, columns] = value.astype(bf16).reshape(plane, slots, chunk)
             if send:
                 give_back(g, c)
             if midway is not None and c == EARLY - 1:
@@ -273,44 +276,48 @@
         gate_val, up_val = pre[:, :part], pre[:, part:]
         hidden_s[g] = (gate_val / (1.0 + jnp.exp(-gate_val)) * up_val).astype(bf16)
 
-    def combined(g, c):
-        columns = pl.ds(c * chunk, chunk)
-        total(brecv.at[g, c], back.at[g, others, :, columns])
-        value = lax.dot_general(
-            pack[g], back[g, :, :, columns].reshape(rows, chunk), (((0,), (0,)), ((), ())),
-            preferred_element_type=f32,
-        )
-        blocks = chunk // sgate_ref.shape[0]
-        first = c * blocks
-        down_t = spread[:, :, :, :, 2 * part :].reshape(width, part)[first * sgate_ref.shape[0] :][
-            :chunk
-        ]
+    def returned(g, c):
+        total(brecv.at[g, c], back.at[g, others, :, pl.ds(c * chunk, chunk)])
+
+    def combined(g, h):
+        columns = pl.ds(h * piece, piece)
+        value = sum(
+            lax.dot_general(
+                unpack[g, i], back[g, :, :, columns].reshape(rows, piece),
+                (((0,), (0,)), ((), ())), preferred_element_type=f32,
+            )
+            for i in range(2)
+        )
+        down_t = spread[:, :, :, :, 2 * part :].reshape(width, part)[h * piece :][:piece]
         return value + lax.dot_general(
             hidden_s[g], down_t, (((1,), (1,)), ((), ())), preferred_element_type=f32
         )
 
-    def land_copy(k, slot, goal, g, c):
-        columns = pl.ds(c * chunk, chunk)
+    def land_copy(slot, goal, g, h):
+        columns = pl.ds(h * piece, piece)
         return pltpu.make_async_remote_copy(
             src_ref=partial.at[g, :, columns], dst_ref=land.at[slot, :, columns],
-            send_sem=lsend.at[0], recv_sem=lrecv.at[slot, c],
+            send_sem=lsend.at[0], recv_sem=lrecv.at[slot, h],
             device_id=(goal * plane + p,), device_id_type=MESH,
         )
 
     def pass_on(k, c, joined=False):
         g = pick(BACK, z, k)
-        columns = pl.ds(c * chunk, chunk)
         slot, goal = pick(SLOT, z, k), pick(GOAL, z, k)
-        value = combined(g, c)
-        if joined:
-            extra = k + 1
-            land_copy(k, jnp.int32(extra), goal, g, c).wait_recv()
-            value += land[extra, :, columns].astype(f32)
-        partial[g, :, columns] = value.astype(bf16)
-        land_copy(k, slot, goal, g, c).start()
+        returned(g, c)
+        for h in range(c * HALVES, (c + 1) * HALVES):
+            columns = pl.ds(h * piece, piece)
+            value = combined(g, h)
+            if joined:
+                extra = k + 1
+                land_copy(jnp.int32(extra), goal, g, h).wait_recv()
+                value += land[extra, :, columns].astype(f32)
+            partial[g, :, columns] = value.astype(bf16)
+            land_copy(slot, goal, g, h).start()
 
     for j in range(1, GROUPS):
-        route_copy(j, z).start()
+        route_copy(j, route.at[p, z], 0).start()
+        route_copy(j, share_of.at[z], 1).start()
     for c in range(CHUNKS):
 
         @pl.when(has_low)
@@ -329,7 +336,8 @@
     for c in range(CHUNKS):
         fill(z, c)
         dispatch(z, c)
-    total(rrecv.at[0], route.at[pl.ds(0, GROUPS - 1), p])
+    total(rrecv.at[0], route.at[p, pl.ds(0, GROUPS - 1)])
+    total(rrecv.at[1], share_of.at[pl.ds(0, GROUPS - 1)])
     for i in range(1, plane):
         route_forward(i, p).start()
     for j in range(1, GROUPS):
@@ -350,7 +358,7 @@
     for goal in near:
         for j in range(1, GROUPS):
             column_copy(goal, (z + j) % GROUPS, chip, 0).start()
-    total(frecv.at[0], route.at[:, others])
+    total(frecv.at[0], route.at[others])
     for copy in weights:
         copy.wait()
     compute(z, False)
@@ -472,16 +480,19 @@
 
     shared_hidden(z)
     for c in range(CHUNKS):
-        columns = pl.ds(c * chunk, chunk)
-        value = combined(z, c)
-        for slot in range(2):
-            land_copy(0, jnp.int32(slot), z, z, c).wait_recv()
-            value += land[slot, :, columns].astype(f32)
-        out_ref[:, columns] = value.astype(out_ref.dtype)
-
-    total(rsend.at[0], route.at[pl.ds(0, GROUPS - 1), p])
+        returned(z, c)
+        for h in range(c * HALVES, (c + 1) * HALVES):
+            columns = pl.ds(h * piece, piece)
+            value = combined(z, h)
+            for slot in range(2):
+                land_copy(jnp.int32(slot), z, z, h).wait_recv()
+                value += land[slot, :, columns].astype(f32)
+            out_ref[:, columns] = value.astype(out_ref.dtype)
+
+    total(rsend.at[0], route.at[p, pl.ds(0, GROUPS - 1)])
+    total(rsend.at[1], share_of.at[pl.ds(0, GROUPS - 1)])
     total(hzsend.at[0], slices.at[pl.ds(0, GROUPS - 1)])
-    total(fsend.at[0], route.at[:, others])
+    total(fsend.at[0], route.at[others])
     total(hpsend.at[0], spread.at[:, pl.ds(0, chips - 1), core])
     core_copy(core).wait_send()
     total(dsend.at[0], packed.at[:, others])
@@ -537,18 +548,20 @@
             pltpu.VMEM(expert_down.shape, bf16),
             pltpu.VMEM(whole, bf16),
             pltpu.VMEM((GROUPS, rows, count_tok), bf16),
+            pltpu.VMEM((GROUPS, 2, rows, count_tok), bf16),
             pltpu.VMEM(blocks, bf16),
             pltpu.VMEM(blocks, bf16),
             pltpu.VMEM(blocks, bf16),
             pltpu.VMEM(whole, bf16),
             pltpu.VMEM(whole, bf16),
-            pltpu.VMEM((GROUPS, plane, 2 * top, count_tok), f32),
+            pltpu.VMEM((plane, GROUPS, top, count_tok), f32),
+            pltpu.VMEM((GROUPS, top, count_tok), f32),
             pltpu.VMEM((GROUPS, depth, 3 * part), bf16),
             pltpu.VMEM((GROUPS, plane // 2, 2, depth, 3 * part), bf16),
             pltpu.VMEM((GROUPS, count_tok, part), bf16),
             dma((3,)),
-            dma((1,)),
-            dma((1,)),
+            dma((2,)),
+            dma((2,)),
             dma((1,)),
             dma((1,)),
             dma((1,)),
@@ -564,7 +577,7 @@
             dma((1,)),
             dma((GROUPS, CHUNKS)),
             dma((1,)),
-            dma((GROUPS, CHUNKS)),
+            dma((GROUPS, CHUNKS * HALVES)),
         ],
         compiler_params=pltpu.CompilerParams(
             collective_id=0, has_side_effects=True, vmem_limit_bytes=52 * 1024 * 1024

time: 86.3 us -> 85.8 us (level)
  no operation moved by 1% of the time
where the time goes in v5:
time: 85.8 us; the launch traced here: 85.7 us
  Pallas kernels  84.9 us (99%)
    pallas_call x1, Pallas kernels, per_device(): pl.pallas_call(functools.partial(moe_kernel, plane, slots, local), out_sh...  84.9 us

profile of v5, /device:TPU:0, one launch (start us, length us, event | category | flops | bytes accessed | tf_op | source)
XLA Modules:
  0.0 85.7 jit_solution(4139716682932978272)
XLA Ops:
  0.0 84.9 %shard_map.100 = bf16[128,2048]{1,0:T(8,128)(2,1)S(1)} custom-call(bf16[128,2048]{1,0:T(8,128)(2,1)} %tok_hbm.1, f32[1,2048]{1,0:T(1,128)} %bitcast.5, s32[4,128]{1,0:T(4,128)} %bitcast.6, f32[4,128]{1,0:T(4,128)} %bitcast.7, bf16[64,512]{1,0:T(8,128)(2,1)} %sgate_hbm.1, bf16[64,512]{1,0:T(8,128)(2,1)} %sup_hbm.1, bf16[64,512]{1,0:T(8,128)(2,1)} %bitcast.4, ...), custom_call_target="tpu_custom_call" | custom-call | tf_op jit(solution)/shard_map/pallas_call | solution.py:532
  84.9 0.8 copy.12

commit v6 on v5

--- a/solution.py
+++ b/solution.py
@@ -463,20 +463,21 @@
     @pl.when(outer)
     def _():
         shared_hidden(three)
+        for c in range(CHUNKS):
+            pass_on(2, c)
         for c in range(EARLY + 1, CHUNKS):
             pass_on(1, c)
-        for c in range(CHUNKS):
-            pass_on(2, c)
         for c in range(EARLY, CHUNKS):
             pass_on(0, c)
 
     @pl.when(middle)
     def _():
         shared_hidden(three)
-        for c in range(EARLY, CHUNKS):
-            pass_on(1, c, True)
+        pass_on(1, EARLY, True)
         for c in range(CHUNKS):
             pass_on(2, c, True)
+        for c in range(EARLY + 1, CHUNKS):
+            pass_on(1, c, True)
 
     shared_hidden(z)
     for c in range(CHUNKS):

time: 85.8 us -> 86.5 us (level)
  no operation moved by 1% of the time
where the time goes in v6:
time: 86.5 us; the launch traced here: 86.4 us
  Pallas kernels  85.6 us (99%)
    pallas_call x1, Pallas kernels, per_device(): pl.pallas_call(functools.partial(moe_kernel, plane, slots, local), out_sh...  85.6 us

profile of v6, /device:TPU:0, one launch (start us, length us, event | category | flops | bytes accessed | tf_op | source)
XLA Modules:
  0.0 86.4 jit_solution(13214411452488294649)
XLA Ops:
  0.0 85.6 %shard_map.100 = bf16[128,2048]{1,0:T(8,128)(2,1)S(1)} custom-call(bf16[128,2048]{1,0:T(8,128)(2,1)} %tok_hbm.1, f32[1,2048]{1,0:T(1,128)} %bitcast.5, s32[4,128]{1,0:T(4,128)} %bitcast.6, f32[4,128]{1,0:T(4,128)} %bitcast.7, bf16[64,512]{1,0:T(8,128)(2,1)} %sgate_hbm.1, bf16[64,512]{1,0:T(8,128)(2,1)} %sup_hbm.1, bf16[64,512]{1,0:T(8,128)(2,1)} %bitcast.4, ...), custom_call_target="tpu_custom_call" | custom-call | tf_op jit(solution)/shard_map/pallas_call | solution.py:533
  85.6 0.8 copy.12
